TPU v7x, 512 devices: a whole 4x4x16 slice. The times are simulated.
512 devices in a mesh: ep: 32 (over z, core), tp: 16 (over y, x).
Axes of the slice: x: 4, y: 4, z: 16, core: 2. Of those that a mesh axis runs over, the one named last changes fastest.
Arguments:
- query_rows: bfloat16 [12288, 2048], P('ep', 'tp'), may hold values from -6 to 6
- key_rows: bfloat16 [12288, 2048], P('ep', 'tp'), may hold values from -6 to 6
- value_rows: bfloat16 [12288, 2048], P('ep', 'tp'), may hold values from -6 to 6
- second_scale: float32 [16], P('tp'), may hold values from 0.3 to 0.8
- head_gain: float32 [128], replicated, may hold values from 0.1 to 1.9
- out_weight: bfloat16 [2048, 4096], P(None, 'tp'), may hold values from -0.125 to 0.125
- routed_rows: bfloat16 [4096, 4096], P('ep', 'tp'), may hold values from -6 to 6
- norm_gain: float32 [4096], replicated, may hold values from 0.1 to 1.9
- route_ids: int32 [4096, 2], P('ep'), may hold values from 0 to 31, all different within a row; in each aligned block of 128 rows (0 to 127, 128 to 255, ...) at most 16 rows name the same one
- route_weight: float32 [4096, 2], P('ep'), may hold values from 0.1 to 0.9
- expert_gate: bfloat16 [32, 4096, 2048], P('ep', None, 'tp'), may hold values from -0.09375 to 0.09375
- expert_up: bfloat16 [32, 4096, 2048], P('ep', None, 'tp'), may hold values from -0.09375 to 0.09375
- expert_down: bfloat16 [32, 2048, 4096], P('ep', None, 'tp'), may hold values from -0.125 to 0.125
Outputs:
- mixer_out: bfloat16 [12288, 4096], P('ep', 'tp')
- expert_mix: bfloat16 [4096, 4096], P('ep', 'tp')
Inputs may be any that keep to these rules, and one draw needn't show every extreme that they name: `route_ids`: among the 128 tokens of one index of ep, no expert is named by more than 16 of them, a bound that some block reaches.
All inputs are finite; a program needn't handle non-finite values.
Results may differ from a plain program's by a relative error of at most 0.0085.
Values may be sent and summed in bfloat16 or wider, within the bound.
A program may use at most 64 MiB of HBM per device.

v0:
```python
import jax
import jax.numpy as jnp
from jax import lax
from jax.sharding import PartitionSpec as P

eps = 1e-06
head_factor = 0.8
neg_big = -1e30
key_block_rows = 1024


def side_by_side(arrays, axis, dim, along):
    both = jnp.concatenate(arrays, axis=along)
    result, at, finished = (lax.all_gather(both, axis, axis=dim, tiled=True), 0, [])
    for a in arrays:
        finished.append(lax.slice_in_dim(result, at, at + a.shape[along], axis=along))
        at += a.shape[along]
    return tuple(finished)


def rms_rows(rows_in, gain):
    floats = rows_in.astype(jnp.float32)
    factor = lax.rsqrt(jnp.mean(floats * floats, axis=-1, keepdims=True) + eps)
    return (floats * factor * gain).astype(jnp.bfloat16)


def per_device(
    query_rows,
    key_rows,
    value_rows,
    second_scale,
    head_gain,
    out_weight,
    routed_rows,
    norm_gain,
    route_ids,
    route_weight,
    expert_gate,
    expert_up,
    expert_down,
):
    count_a = query_rows.shape[0]
    per_head = second_scale.shape[0]
    head_dim = query_rows.shape[1] // (2 * per_head)
    value_dim = head_gain.shape[0]
    query_four = query_rows.reshape(count_a, per_head, 2, head_dim)
    query_pos = lax.axis_index("ep") * count_a + jnp.arange(count_a, dtype=jnp.int32)

    def key_block(carry_state, key_part, value_part, block_start):
        key_count = key_part.shape[0]
        key_four = key_part.reshape(key_count, per_head, 2, head_dim)
        value_three = value_part.reshape(key_count, per_head, value_dim)
        scores = jnp.einsum(
            "ihcd,jhcd->ihcj", query_four, key_four, preferred_element_type=jnp.float32
        ) * head_dim ** (-0.5)
        allowed = (
            query_pos[:, None] >= block_start + jnp.arange(key_count, dtype=jnp.int32)[None, :]
        )[:, None, None, :]
        scores = jnp.where(allowed, scores, neg_big)
        old_max, old_sum, old_acc = carry_state
        new_max = jnp.maximum(old_max, jnp.max(scores, axis=-1))
        weights = jnp.where(allowed, jnp.exp(scores - new_max[..., None]), 0.0)
        shrink = jnp.exp(old_max - new_max)
        new_sum = old_sum * shrink + jnp.sum(weights, axis=-1)
        update = jnp.einsum(
            "ihcj,jhe->ihce",
            weights.astype(jnp.bfloat16),
            value_three,
            preferred_element_type=jnp.float32,
        )
        return (new_max, new_sum, old_acc * shrink[..., None] + update)

    start_state = (
        jnp.full((count_a, per_head, 2), neg_big, jnp.float32),
        jnp.zeros((count_a, per_head, 2), jnp.float32),
        jnp.zeros((count_a, per_head, 2, value_dim), jnp.float32),
    )
    key_part, value_part = side_by_side((key_rows, value_rows), "ep", 0, 1)
    key_count = key_part.shape[0]

    def step_block(block_num, inner_state):
        offset_rows = block_num * key_block_rows
        key_slice = lax.dynamic_slice_in_dim(key_part, offset_rows, key_block_rows, 0)
        value_slice = lax.dynamic_slice_in_dim(value_part, offset_rows, key_block_rows, 0)
        return key_block(inner_state, key_slice, value_slice, offset_rows)

    run_max, run_sum, run_acc = lax.fori_loop(
        0, key_count // key_block_rows, step_block, start_state
    )
    maps_both = run_acc / run_sum[..., None]
    mixed_maps = maps_both[:, :, 0] - second_scale[None, :, None] * maps_both[:, :, 1]
    mean_sq = jnp.mean(mixed_maps * mixed_maps, axis=-1, keepdims=True)
    head_out = (
        (mixed_maps * lax.rsqrt(mean_sq + eps) * head_gain * head_factor)
        .astype(jnp.bfloat16)
        .reshape(count_a, per_head * value_dim)
    )
    count_b = routed_rows.shape[0]
    route_count = route_ids.shape[1]
    experts_here = expert_gate.shape[0]
    ep_devices = lax.axis_size("ep")
    expert_total = experts_here * ep_devices
    capacity = 2 * count_b * route_count // expert_total
    flat_expert = route_ids.reshape(-1)
    chosen = (flat_expert[:, None] == jnp.arange(expert_total, dtype=jnp.int32)[None, :]).astype(
        jnp.int32
    )
    ranks = jnp.sum((jnp.cumsum(chosen, axis=0) - 1) * chosen, axis=1)
    slot_of = flat_expert * capacity + ranks
    token_of = jnp.arange(count_b * route_count, dtype=jnp.int32) // route_count
    slot_token = jnp.full((expert_total * capacity,), count_b, jnp.int32).at[slot_of].set(token_of)
    padded = jnp.concatenate(
        [routed_rows, jnp.zeros((1, routed_rows.shape[1]), jnp.bfloat16)], axis=0
    )
    outgoing = padded[slot_token].reshape(ep_devices, experts_here, capacity, routed_rows.shape[1])
    column_parts = lax.all_to_all(outgoing, "ep", split_axis=0, concat_axis=0, tiled=True)
    arrived = rms_rows(lax.all_gather(column_parts, "tp", axis=3, tiled=True), norm_gain)
    gate_val = jnp.einsum(
        "sxcd,xdf->sxcf", arrived, expert_gate, preferred_element_type=jnp.float32
    )
    up_val = jnp.einsum("sxcd,xdf->sxcf", arrived, expert_up, preferred_element_type=jnp.float32)
    hidden = (jax.nn.silu(gate_val) * up_val).astype(jnp.bfloat16)
    weight_rows = out_weight
    attn_total = jnp.dot(
        lax.all_gather(
            head_out.reshape(1, 1, count_a, head_out.shape[1]), "tp", axis=3, tiled=True
        )[0, 0],
        weight_rows,
        preferred_element_type=jnp.float32,
    )
    weight_rows = expert_down
    moe_total = jnp.einsum(
        "sxcf,xfd->sxcd",
        lax.all_gather(hidden, "tp", axis=3, tiled=True),
        weight_rows,
        preferred_element_type=jnp.float32,
    )
    mixer_out = attn_total.astype(jnp.bfloat16)
    returned = lax.all_to_all(
        moe_total.astype(jnp.bfloat16), "ep", split_axis=0, concat_axis=0, tiled=True
    )
    flat_back = returned.reshape(expert_total * capacity, returned.shape[3])
    picked = flat_back[slot_of].astype(jnp.float32).reshape(count_b, route_count, returned.shape[3])
    expert_mix = jnp.sum(picked * route_weight[:, :, None], axis=1).astype(jnp.bfloat16)
    return (mixer_out, expert_mix)


def solution(mesh):
    placed = (
        P("ep", "tp"),
        P("ep", "tp"),
        P("ep", "tp"),
        P("tp"),
        P(),
        P(None, "tp"),
        P("ep", "tp"),
        P(),
        P("ep", None),
        P("ep", None),
        P("ep", None, "tp"),
        P("ep", None, "tp"),
        P("ep", None, "tp"),
    )
    return jax.shard_map(
        per_device,
        mesh=mesh,
        in_specs=placed,
        out_specs=(P("ep", "tp"), P("ep", "tp")),
        check_vma=False,
    )
```

profile of v0, /device:TPU:1, one launch (start us, length us, event | category | flops | bytes accessed | tf_op | source)
XLA Modules:
  0.0 361.5 jit_solution(12429718926275836795)
XLA Ops:
  14.6 39.0 %all_to_all.10 = bf16[32,1,16,256]{3,2,1,0:T(8,128)(2,1)} all-to-all(bf16[32,1,16,256]{3,2,1,0:T(8,128)(2,1)S(1)} %bitcast.173), channel_id=1, replica_groups=mesh['ep'=32,'tp'=16] {'ep'}, dimensions={0} | all-to-all | bytes 524288 | tf_op jit(solution)/shard_map/all_to_all | solution.py:116
  55.5 60.3 %all-gather.9.cloned.1.call-done = bf16[32,1,16,4096]{3,2,1,0:T(8,128)(2,1)} async-done(((bf16[32,1,16,256]{3,2,1,0:T(8,128)(2,1)}), bf16[32,1,16,4096]{3,2,1,0:T(8,128)(2,1)}) %all-gather.9.cloned.1.call-update) | async-done | bytes 4194320 | tf_op jit(solution)/shard_map/all_gather | solution.py:117
  115.9 3.2 fusion.24
  122.6 73.7 %all-gather.5.cloned.1.call-done = bf16[12288,256]{0,1:T(8,128)(2,1)} async-done(((bf16[384,256]{0,1:T(8,128)(2,1)}), bf16[12288,256]{0,1:T(8,128)(2,1)}) %all-gather.5.cloned.1.call-update) | async-done | bytes 6291472 | tf_op jit(solution)/shard_map/all_gather | solution.py:14
  196.4 6.2 %fusion.69 = (bf16[12288,128]{0,1:T(8,128)(2,1)}, bf16[12288,128]{0,1:T(8,128)(2,1)}) fusion(bf16[12288,256]{0,1:T(8,128)(2,1)} %all-gather.5.cloned.1.call-done), kind=kLoop, calls=%fused_computation.86 | loop fusion | bytes 12582912 | tf_op jit(solution)/shard_map/slice | solution.py:16
  202.6 94.7 %while.18 = (s32[]{:T(128)}, f32[384,1,2]{0,2,1:T(2,128)S(1)}, f32[384,1,2]{0,2,1:T(2,128)S(1)}, f32[384,1,2,128]{0,3,2,1:T(8,128)S(1)}, bf16[12288,128]{0,1:T(8...) while((s32[]{:T(128)}, f32[384,1,2]{0,2,1:T(2,128)S(1)}, ...), condition=%wide.region_3.4_spmd.clone, body=%wide.region_0.3_spmd.clone.sunk | while | flops 312907648 | bytes 25586904 | solution.py:87
  203.8 2.4 fusion.82
  206.3 3.2 fusion.85
  211.7 2.4 fusion.82
  214.2 3.2 fusion.85
  219.6 2.4 fusion.82
  222.1 3.2 fusion.85
  227.5 2.4 fusion.82
  230.0 3.2 fusion.85
  235.4 2.4 fusion.82
  237.9 3.2 fusion.85
  243.3 2.4 fusion.82
  245.8 3.2 fusion.85
  253.6 3.3 fusion.85
  259.1 2.4 fusion.82
  261.6 3.2 fusion.85
  269.5 3.2 fusion.85
  274.9 2.4 fusion.82
  277.4 3.2 fusion.85
  285.3 3.2 fusion.85
  290.7 2.4 fusion.82
  293.2 3.2 fusion.85
  298.2 3.1 fusion.48
  301.3 7.9 %all-to-all-start.1 = ((bf16[32,1,16,256]{3,2,1,0:T(8,128)(2,1)}), bf16[32,1,16,256]{3,2,1,0:T(8,128)(2,1)S(1)}, u32[]{:S(2)}, u32[]{:S(2)}) async-start(bf16[32,1,16,256]{3,2,1,0:T(8,128)(2,1)} %fusion.48), calls=%async_computation.1 | async-start | bytes 524288 | tf_op jit(solution)/shard_map/all_to_all | solution.py:139
  309.4 22.1 %all-to-all-done.1 = bf16[32,1,16,256]{3,2,1,0:T(8,128)(2,1)S(1)} async-done(((bf16[32,1,16,256]{3,2,1,0:T(8,128)(2,1)}), bf16[32,1,16,256]{3,2,1,0:T(8,128)(2,1)S(1)}, u32[]{:S(2)}, u32[]{:S(2)}) %all-to-all-start.1) | async-done | bytes 262176 | tf_op jit(solution)/shard_map/all_to_all | solution.py:139
  333.8 18.4 %all-gather.7.cloned.1.call-done = bf16[1,1,384,2048]{2,3,1,0:T(8,128)(2,1)} async-done(((bf16[1,1,384,128]{2,3,1,0:T(8,128)(2,1)}), bf16[1,1,384,2048]{2,3,1,0:T(8,128)(2,1)}) %all-gather.7.cloned.1.call-update) | async-done | bytes 1572880 | tf_op jit(solution)/shard_map/all_gather | solution.py:125
  352.3 2.7 fusion.39
  (192 shorter events, 48.4 us)
Async XLA Ops:
  7.2 291.1 %copy-start = (bf16[1,2048,256]{2,1,0:T(8,128)(2,1)S(1)}, bf16[1,2048,256]{2,1,0:T(8,128)(2,1)}, u32[]{:S(2)}) copy-start(bf16[1,2048,256]{2,1,0:T(8,128)(2,1)} %param.27) | copy-start | bytes 3145732
  7.2 46.5 %copy-start.4 = (bf16[384,128]{1,0:T(8,128)(2,1)S(1)}, bf16[384,128]{1,0:T(8,128)(2,1)}, u32[]{:S(2)}) copy-start(bf16[384,128]{1,0:T(8,128)(2,1)} %param.16) | copy-start | bytes 294916
  7.2 46.6 %copy-start.5 = (bf16[384,128]{1,0:T(8,128)(2,1)S(1)}, bf16[384,128]{1,0:T(8,128)(2,1)}, u32[]{:S(2)}) copy-start(bf16[384,128]{1,0:T(8,128)(2,1)} %param.17) | copy-start | bytes 294916
  7.2 47.6 %copy-start.6 = (bf16[384,128]{1,0:T(8,128)(2,1)S(1)}, bf16[384,128]{1,0:T(8,128)(2,1)}, u32[]{:S(2)}) copy-start(bf16[384,128]{1,0:T(8,128)(2,1)} %param.15) | copy-start | bytes 294916
  7.2 108.6 %all-gather.9.cloned.1.call-start = ((), (), s32[]{:S(2)}) async-start(), calls=%async_computation.4 | async-start | bytes 4456448 | tf_op jit(solution)/shard_map/all_gather | solution.py:117
  14.5 104.6 %copy-start.9 = (bf16[1,4096,128]{2,1,0:T(8,128)(2,1)S(1)}, bf16[1,4096,128]{2,1,0:T(8,128)(2,1)}, u32[]{:S(2)}) copy-start(bf16[1,4096,128]{2,1,0:T(8,128)(2,1)} %param.25) | copy-start | bytes 3145732
  14.5 104.6 %copy-start.11 = (f32[4096]{0:T(1024)S(1)}, f32[4096]{0:T(1024)}, u32[]{:S(2)}) copy-start(f32[4096]{0:T(1024)} %param.22) | copy-start | bytes 49156
  53.6 142.8 %all-gather.5.cloned.1.call-start = ((), (), s32[]{:S(2)}) async-start(), calls=%async_computation.2 | async-start | bytes 6488064 | tf_op jit(solution)/shard_map/all_gather | solution.py:14
  54.7 243.5 %all-gather.11.cloned.1.call-start = ((), (), s32[]{:S(2)}) async-start(), calls=%async_computation.5 | async-start | bytes 2228224 | tf_op jit(solution)/shard_map/all_gather | solution.py:134
  115.8 3.4 copy-start.2
  119.3 1.3 copy-start.10
  122.6 229.7 %all-gather.7.cloned.1.call-start = ((), (), s32[]{:S(2)}) async-start(), calls=%async_computation.3 | async-start | bytes 1671168 | tf_op jit(solution)/shard_map/all_gather | solution.py:125
  202.6 94.9 %copy-start.8 = (f32[128]{0:T(128)S(1)}, f32[128]{0:T(128)}, u32[]{:S(2)}) copy-start(f32[128]{0:T(128)} %param.19) | copy-start | bytes 1540
  206.3 3.3 copy-start.1
  214.2 3.3 copy-start.1
  222.1 3.3 copy-start.1
  230.0 3.3 copy-start.1
  237.9 3.3 copy-start.1
  245.7 3.3 copy-start.1
  253.6 3.3 copy-start.1
  261.6 3.3 copy-start.1
  269.5 3.3 copy-start.1
  277.4 3.3 copy-start.1
  285.3 3.3 copy-start.1
  293.1 3.3 copy-start.1
  297.3 12.0 %copy-start.7 = (f32[128,2]{0,1:T(2,128)S(1)}, f32[128,2]{0,1:T(2,128)}, u32[]{:S(2)}) copy-start(f32[128,2]{0,1:T(2,128)} %param.24) | copy-start | bytes 3076
  298.2 54.1 %copy-start.3 = (bf16[2048,256]{1,0:T(8,128)(2,1)S(1)}, bf16[2048,256]{1,0:T(8,128)(2,1)}, u32[]{:S(2)}) copy-start(bf16[2048,256]{1,0:T(8,128)(2,1)} %param.20) | copy-start | bytes 3145732
  301.3 30.2 %all-to-all-start.1 = ((bf16[32,1,16,256]{3,2,1,0:T(8,128)(2,1)}), bf16[32,1,16,256]{3,2,1,0:T(8,128)(2,1)S(1)}, u32[]{:S(2)}, u32[]{:S(2)}) async-start(bf16[32,1,16,256]{3,2,1,0:T(8,128)(2,1)} %fusion.48), calls=%async_computation.1 | async-start | bytes 524288 | tf_op jit(solution)/shard_map/all_to_all | solution.py:139
Sparse Core Ops, SparseCore 0:
  53.7 62.0 all-gather.8
  118.5 77.8 all-gather.4
  199.4 56.9 all-gather.10
  298.3 53.9 all-gather.6
where the time goes:
time: 362 us
  waiting for transfers between devices  175 us (48%)
  matrix products  77 us (21%)
  blocking collectives  39 us (11%)
  local copies, waits for them, and re-layouts  25.7 us (7%)
  other arithmetic  21.3 us (6%)
  between operations  14.7 us (4%)
  starting transfers between devices  8.09 us (2%)
    all_gather x1, waiting for transfers between devices, side_by_side(): lax.all_gather(both, axis, axis=dim, tiled=True)  73.7 us
    all_gather x1, waiting for transfers between devices, per_device(): lax.all_gather(column_parts, 'tp', axis=3, tiled=True)  60.3 us
    all_to_all x1, blocking collectives, per_device(): lax.all_to_all(outgoing, 'ep', split_axis=0, concat_axis=0, tiled=True)  39 us
    dot_general x12, matrix products, key_block(): jnp.einsum('ihcj,jhe->ihce', weights.astype(jnp.bfloat16), value_three, p...  38.9 us
    dot_general x12, matrix products, key_block(): jnp.einsum('ihcd,jhcd->ihcj', query_four, key_four, preferred_element_typ...  29.1 us
    all_to_all x1, waiting for transfers between devices, per_device(): lax.all_to_all(moe_total.astype(jnp.bfloat16), 'ep', split_axis=0, concat...  22.1 us
    all_gather x1, waiting for transfers between devices, per_device(): lax.all_gather(head_out.reshape(1, 1, count_a, head_out.shape[1]), 'tp',...  18.4 us
    dynamic_slice x12, local copies, waits for them, and re-layouts, step_block(): lax.dynamic_slice_in_dim(key_part, offset_rows, key_block_rows, 0)  11.7 us
  transfers between devices with their start and end apart: 5, of which 4 were waited for; matrix products, arithmetic and copies ran while one was open for 31% of the time, Pallas kernels for 0%

commit v1 on v0

v1 whole, which is shorter than its diff:
```python
import functools
import math

import jax
import jax.numpy as jnp
from jax import lax
from jax.experimental import pallas as pl
from jax.experimental.pallas import tpu as pltpu
from jax.sharding import PartitionSpec as P

MESH = pl.DeviceIdType.MESH
F32 = jnp.float32
BF16 = jnp.bfloat16
EPS = 1e-06
HEAD_FACTOR = 0.8
NEG = -1e30
PLANE = {16: (4, 4), 1: (1, 1)}


def dot(a, b):
    return lax.dot_general(a, b, (((1,), (0,)), ((), ())), preferred_element_type=F32)


def kernel(
    nz,
    ny,
    nx,
    cap,
    q_ref,
    k_ref,
    v_ref,
    scale_ref,
    hgain_ref,
    wout_hbm,
    x_ref,
    ngain_ref,
    ids_ref,
    rw_ref,
    gate_hbm,
    up_hbm,
    down_hbm,
    mixer_ref,
    mix_ref,
    kbuf,
    vbuf,
    qq,
    m_ref,
    acc,
    ssbuf,
    disp,
    xbuf,
    gu,
    hbuf,
    obuf,
    rbuf,
    hobuf,
    picks,
    wgu,
    wdown,
    wout,
    w_sem,
    own_send,
    own_recv,
    ring_send,
    ring_recv,
    pass_send,
    pass_recv,
    ss_send,
    ss_recv,
    a2a_send,
    a2a_recv,
    xy_send,
    xy_recv,
):
    n_ep, n_tp = 2 * nz, ny * nx
    ta, hd2 = q_ref.shape
    vd = v_ref.shape[1]
    tb, dcol = x_ref.shape
    slots = n_ep * cap
    ff = gate_hbm.shape[1]
    ocol = wdown.shape[1]
    steps = nz // 2

    ep = lax.axis_index("ep")
    tp = lax.axis_index("tp")
    z, c = lax.div(ep, 2), lax.rem(ep, 2)
    y, x = lax.div(tp, nx), lax.rem(tp, nx)

    def at_ep(zz, cc):
        return {"ep": 2 * zz + cc}

    def remote(src, dst, ssem, rsem, dev):
        return pltpu.make_async_remote_copy(
            src_ref=src, dst_ref=dst, send_sem=ssem, recv_sem=rsem, device_id=dev, device_id_type=MESH
        )

    barrier = pltpu.get_barrier_semaphore()

    def greet_ep(i, carry):
        pl.semaphore_signal(barrier, inc=1, device_id={"ep": lax.rem(ep + i, n_ep)}, device_id_type=MESH)
        return carry

    def greet_tp(i, carry):
        pl.semaphore_signal(barrier, inc=1, device_id={"tp": lax.rem(tp + i, n_tp)}, device_id_type=MESH)
        return carry

    lax.fori_loop(1, n_ep, greet_ep, 0)
    if n_tp > 1:
        lax.fori_loop(1, n_tp, greet_tp, 0)

    w_copies = [
        pltpu.make_async_copy(gate_hbm, wgu.at[:, pl.ds(0, ff)], w_sem.at[0]),
        pltpu.make_async_copy(up_hbm, wgu.at[:, pl.ds(ff, ff)], w_sem.at[1]),
        pltpu.make_async_copy(down_hbm, wdown, w_sem.at[2]),
        pltpu.make_async_copy(wout_hbm, wout, w_sem.at[3]),
    ]
    for copy in w_copies:
        copy.start()

    v_t = v_ref[...].astype(F32).T.astype(BF16)

    @pl.when(c == 0)
    def _():
        vbuf[z, 0:vd, 0:ta] = v_t

    @pl.when(c == 1)
    def _():
        vbuf[z, 0:vd, ta : 2 * ta] = v_t

    kbuf[ep] = k_ref[...]
    x_own = x_ref[...].astype(F32)
    squares = jnp.sum((x_own * x_own).T, axis=0, keepdims=True)
    ssbuf[tp] = jnp.broadcast_to(squares, (8, tb))

    def ones_rows(i, carry):
        vbuf[i, vd : vd + 16, :] = jnp.ones((16, 2 * ta), BF16)
        return carry

    lax.fori_loop(0, nz, ones_rows, 0)

    half = hd2 // 2
    q_t = (q_ref[...].astype(F32) * (math.log2(math.e) * half**-0.5)).T
    q_hi = q_t.astype(BF16)
    q_lo = (q_t - q_hi.astype(F32)).astype(BF16)
    none = jnp.zeros((half, ta), BF16)
    for i, part in enumerate((q_hi, q_lo)):
        qq[2 * half * i : 2 * half * i + half, 0:ta] = part[0:half]
        qq[2 * half * i : 2 * half * i + half, ta : 2 * ta] = none
        qq[2 * half * i + half : 2 * half * (i + 1), 0:ta] = none
        qq[2 * half * i + half : 2 * half * (i + 1), ta : 2 * ta] = part[half:]
    m_ref[...] = jnp.full(m_ref.shape, NEG, F32)
    acc[...] = jnp.zeros(acc.shape, F32)

    ids = ids_ref[...]
    lane = lax.broadcasted_iota(jnp.int32, (tb, 128), 1)
    first = jnp.where(ids[:, 0:1] == lane, 1.0, 0.0).astype(F32)
    second = jnp.where(ids[:, 1:2] == lane, 1.0, 0.0).astype(F32)
    lower = jnp.where(
        lax.broadcasted_iota(jnp.int32, (tb, tb), 0) > lax.broadcasted_iota(jnp.int32, (tb, tb), 1), 1.0, 0.0
    ).astype(BF16)
    before_0 = dot(lower, first.astype(BF16))
    before_1 = dot(lower, second.astype(BF16)) + jnp.sum(first, axis=0, keepdims=True)
    rank_0 = jnp.sum(first * before_0, axis=1, keepdims=True)
    rank_1 = jnp.sum(second * before_1, axis=1, keepdims=True)
    slot_0 = ids[:, 0:1].astype(F32) * cap + rank_0
    slot_1 = ids[:, 1:2].astype(F32) * cap + rank_1
    slot_lane = lax.broadcasted_iota(jnp.int32, (tb, slots), 1).astype(F32)
    pick_0 = jnp.where(slot_0 == slot_lane, 1.0, 0.0).astype(F32)
    pick_1 = jnp.where(slot_1 == slot_lane, 1.0, 0.0).astype(F32)
    picks[0] = pick_0.astype(BF16)
    picks[1] = pick_1.astype(BF16)
    spread = (pick_0 + pick_1).T.astype(BF16)

    pl.semaphore_wait(barrier, (n_ep - 1) + (n_tp - 1))

    def k_at(zz, cc):
        return kbuf.at[2 * zz + cc]

    def v_at(zz, cc):
        return vbuf.at[zz, pl.ds(0, vd), pl.ds(pl.multiple_of(cc * ta, 128), ta)]

    part_at = (k_at, v_at)

    def wrap(zz):
        return lax.rem(zz + nz, nz)

    def hop(direction, s, kv, owner):
        ref = part_at[kv](owner, c)
        to = wrap(z + 1) if direction == 0 else wrap(z - 1)
        return remote(
            ref, ref, ring_send.at[direction, s, kv], ring_recv.at[direction, s, kv], at_ep(to, c)
        )

    def handover(direction, s, kv, owner):
        ref = part_at[kv](owner, c)
        return remote(
            ref, ref, pass_send.at[direction, s, kv], pass_recv.at[direction, s, kv], at_ep(z, 1 - c)
        )

    def handed(direction, s, kv, owner):
        ref = part_at[kv](owner, 1 - c)
        return remote(
            ref, ref, pass_send.at[direction, s, kv], pass_recv.at[direction, s, kv], at_ep(z, 1 - c)
        )

    def owner_of(direction, s):
        return wrap(z - s) if direction == 0 else wrap(z + s)

    last = (steps, nz - 1 - steps)
    for kv in range(2):
        for direction in range(2):
            if last[direction] >= 1:
                hop(direction, 1, kv, z).start()
        handover(0, 0, kv, z).start()

    def ring_tick(s):
        for direction in range(2):

            @pl.when(s <= last[direction])
            def _(direction=direction):
                for kv in range(2):
                    owner = owner_of(direction, s)
                    hop(direction, s, kv, owner).wait_recv()

                    @pl.when(s < last[direction])
                    def _(direction=direction, kv=kv, owner=owner):
                        hop(direction, s + 1, kv, owner).start()

                    handover(direction, s, kv, owner).start()

    n_tile = 256 if (2 * ta) % 256 == 0 else 2 * ta

    def attend(owner, masked):
        keys = kbuf[pl.ds(2 * owner, 2)].reshape(2 * ta, hd2)
        keys = jnp.concatenate([keys, keys], axis=1)
        values = vbuf[owner]
        for n in range(2 * ta // n_tile):
            cols = slice(n * n_tile, (n + 1) * n_tile)
            s = dot(keys, qq[:, cols])
            if masked:
                row = lax.broadcasted_iota(jnp.int32, s.shape, 0)
                col = lax.broadcasted_iota(jnp.int32, s.shape, 1) + n * n_tile
                col = jnp.where(col >= ta, col - ta, col) + c * ta
                s = jnp.where(row <= col, s, NEG)
            old = m_ref[:, cols]
            new = jnp.maximum(old, jnp.max(s, axis=0, keepdims=True))
            weights = jnp.exp2(s - new).astype(BF16)
            shrink = jnp.exp2(old - new)
            m_ref[:, cols] = new
            acc[:, cols] = acc[:, cols] * shrink + dot(values, weights)

    def ss_copy(i):
        peer = lax.rem(tp + i, n_tp)
        return remote(ssbuf.at[tp], ssbuf.at[tp], ss_send.at[i], ss_recv.at[i], {"tp": peer})

    def ss_from(i):
        ref = ssbuf.at[lax.rem(tp - i + n_tp, n_tp)]
        return remote(ref, ref, ss_send.at[i], ss_recv.at[i], {"tp": lax.rem(tp + i, n_tp)})

    def loop(lo, hi, f):
        if hi > lo:
            lax.fori_loop(lo, hi, lambda i, carry: (f(i), carry)[1], 0)

    loop(1, n_tp, lambda i: ss_copy(i).start())

    for kv in range(2):
        handed(0, 0, kv, z).wait_recv()
    attend(z, True)

    loop(1, n_tp, lambda i: ss_from(i).wait_recv())
    total = ssbuf[0, 0:1, :]
    for i in range(1, n_tp):
        total = total + ssbuf[i, 0:1, :]
    factor = lax.rsqrt(total / (n_tp * dcol) + EPS)
    factor = jnp.broadcast_to(factor, (128, tb)).T
    factor = jnp.concatenate([factor] * (dcol // 128), axis=1)
    gain = ngain_ref[:, pl.ds(pl.multiple_of(tp * dcol, 128), dcol)]
    normed = (x_ref[...].astype(F32) * factor * gain).astype(BF16)
    disp[...] = dot(spread, normed).astype(BF16)

    def dispatch_copy(peer):
        return remote(
            disp.at[pl.ds(pl.multiple_of(peer * cap, cap), cap)],
            xbuf.at[tp, pl.ds(pl.multiple_of(ep * cap, cap), cap)],
            a2a_send.at[0, peer],
            a2a_recv.at[0, ep],
            {"ep": peer},
        )

    def dispatched(source):
        return remote(
            disp.at[pl.ds(pl.multiple_of(source * cap, cap), cap)],
            xbuf.at[tp, pl.ds(pl.multiple_of(source * cap, cap), cap)],
            a2a_send.at[0, source],
            a2a_recv.at[0, source],
            {"ep": source},
        )

    def return_copy(peer):
        return remote(
            obuf.at[pl.ds(pl.multiple_of(peer * cap, cap), cap)],
            rbuf.at[pl.ds(pl.multiple_of(ep * cap, cap), cap)],
            a2a_send.at[1, peer],
            a2a_recv.at[1, ep],
            {"ep": peer},
        )

    def returned(source):
        return remote(
            obuf.at[pl.ds(pl.multiple_of(source * cap, cap), cap)],
            rbuf.at[pl.ds(pl.multiple_of(source * cap, cap), cap)],
            a2a_send.at[1, source],
            a2a_recv.at[1, source],
            {"ep": source},
        )

    def others(f):
        def each(i):
            chip, core = lax.div(i, 2), lax.rem(i, 2)
            d = steps - lax.div(chip + 1, 2)
            zz = lax.rem(jnp.where(lax.rem(chip, 2) == 1, z + d, z - d + nz), nz)
            f(2 * zz + core)

        if nz > 1:
            loop(0, 2 * (nz - 1), each)
        f(2 * z + 1 - c)

    others(lambda peer: dispatch_copy(peer).start())
    mine = pl.ds(pl.multiple_of(ep * cap, cap), cap)
    xbuf[tp, mine, :] = disp[mine, :]

    def plane_gather(number, rows, block):
        quarter = rows // 2

        def half_stages(h):
            size_p, size_s = (nx, ny) if h == 0 else (ny, nx)
            p, s = (x, y) if h == 0 else (y, x)

            def index(ss, pp):
                ss, pp = lax.rem(ss + 4, 4), lax.rem(pp + 4, 4)
                return ss * nx + pp if h == 0 else pp * nx + ss

            rel = (0, -1, 1, 2)
            whole, low, high = (0, rows), (0, quarter), (quarter, quarter)

            def msg(name, ds, dp, part):
                sem = {"pr": 0, "pl": 1, "fr": 2, "fl": 3}.get(name)
                if sem is None:
                    sem = 4 + 4 * ("su", "sd", "gu", "gd").index(name[:2]) + int(name[2])
                ts, tp_ = {
                    "pr": (0, 1), "pl": (0, -1), "fr": (0, 1), "fl": (0, -1),
                    "su": (1, 0), "sd": (-1, 0), "gu": (1, 0), "gd": (-1, 0),
                }[name if sem < 4 else name[:2]]
                ref = block(h, index(s + ds, p + dp), *part)
                return remote(
                    ref, ref, xy_send.at[number, h, sem], xy_recv.at[number, h, sem], {"tp": index(s + ts, p + tp_)}
                )

            sent = []

            def send(name, ds, dp, part):
                msg(name, ds, dp, part).start()
                sent.append(lambda: msg(name, ds, dp, part).wait_send())

            def out(j):
                send(f"su{j}", 0, rel[j], whole)
                send(f"sd{j}", 0, rel[j], whole)

            def forward(j):
                msg(f"su{j}", -1, rel[j], whole).wait_recv()
                send(f"gu{j}", -1, rel[j], low)
                msg(f"sd{j}", 1, rel[j], whole).wait_recv()
                send(f"gd{j}", 1, rel[j], high)

            def ended(j):
                msg(f"gu{j}", -2, rel[j], low).wait_recv()
                msg(f"gd{j}", 2, rel[j], high).wait_recv()

            def stage0():
                send("pr", 0, 0, whole)
                send("pl", 0, 0, whole)
                out(0)

            def stage1():
                msg("pr", 0, -1, whole).wait_recv()
                send("fr", 0, -1, low)
                out(1)
                msg("pl", 0, 1, whole).wait_recv()
                send("fl", 0, 1, high)
                out(2)

            def stage2():
                msg("fr", 0, -2, low).wait_recv()
                msg("fl", 0, 2, high).wait_recv()
                out(3)
                forward(0)

            def stage3():
                forward(1)
                forward(2)

            def stage4():
                forward(3)
                for j in range(3):
                    ended(j)

            def stage5():
                ended(3)

            return (stage0, stage1, stage2, stage3, stage4, stage5), sent

        if n_tp == 1:
            return [lambda: None] * 6, lambda: None
        (a, sent_a), (b, sent_b) = half_stages(0), half_stages(1)

        def both(i):
            a[i]()
            b[i]()

        def drained():
            for wait in sent_a + sent_b:
                wait()

        return [functools.partial(both, i) for i in range(6)], drained

    rows_x = slots // 2

    def x_block(h, owner, row, count):
        return xbuf.at[owner, pl.ds(h * rows_x + row, count)]

    def h_block(h, owner, row, count):
        return hbuf.at[pl.ds(h * rows_x + row, count), pl.ds(pl.multiple_of(owner * ff, 128), ff)]

    rows_a = ta // 2

    def ho_block(h, owner, row, count):
        return hobuf.at[pl.ds(h * rows_a + row, count), pl.ds(pl.multiple_of(owner * vd, 128), vd)]

    x_stages, x_sent = plane_gather(0, rows_x, x_block)
    h_stages, h_sent = plane_gather(1, rows_x, h_block)
    o_stages, o_sent = plane_gather(2, rows_a, ho_block)

    def arrive():
        def wait(i):
            dispatched(lax.rem(ep + i, n_ep)).wait_recv()

        loop(1, n_ep, wait)
        x_stages[0]()

    def experts():
        w_copies[0].wait()
        w_copies[1].wait()
        gu[...] = jnp.zeros(gu.shape, F32)

        def block(t):
            gu[...] += dot(xbuf[t], wgu[pl.ds(pl.multiple_of(t * dcol, dcol), dcol), :])

        loop(0, n_tp, block)
        gate, up = gu[:, 0:ff], gu[:, ff : 2 * ff]
        hidden = (gate / (1.0 + jnp.exp(-gate)) * up).astype(BF16)
        hbuf[:, pl.ds(pl.multiple_of(tp * ff, 128), ff)] = hidden

    def x_last():
        x_stages[5]()
        experts()
        h_stages[0]()

    def h_later():
        h_stages[3]()
        h_stages[4]()

    stages = [
        arrive,
        x_stages[1],
        x_stages[2],
        x_stages[3],
        x_stages[4],
        x_last,
        h_stages[1],
        h_stages[2],
        h_later,
    ]

    def pairs(s):
        def one(direction):
            owner_z = jnp.where(direction == 0, z - s, z + s - nz)

            @pl.when(jnp.logical_and(owner_z >= 0, s <= jnp.where(direction == 0, last[0], last[1])))
            def _():
                attend(owner_z, False)

        for direction in range(2):

            @pl.when(jnp.logical_and(s >= 1, s <= last[direction]))
            def _(direction=direction):
                for kv in range(2):
                    handed(direction, s, kv, owner_of(direction, s)).wait_recv()

        @pl.when(s >= 1)
        def _():
            loop(0, 2, one)

    def tick(s):
        ring_tick(s)
        for i, stage in enumerate(stages):
            if i + 1 <= steps + 1:
                pl.when(s == i + 1)(stage)
        pairs(s - 1)

    loop(1, steps + 2, tick)
    for stage in stages[steps + 1 :]:
        stage()

    maps = acc[0:vd, :] / acc[vd : vd + 1, :]
    mixed = maps[:, 0:ta] - scale_ref[0] * maps[:, ta : 2 * ta]
    mean_sq = jnp.mean(mixed * mixed, axis=0, keepdims=True)
    head = (mixed * lax.rsqrt(mean_sq + EPS)).T * hgain_ref[...] * HEAD_FACTOR
    hobuf[:, pl.ds(pl.multiple_of(tp * vd, 128), vd)] = head.astype(BF16)
    o_stages[0]()

    h_stages[5]()
    w_copies[2].wait()
    obuf[...] = dot(hbuf[...], wdown[...]).astype(BF16)
    others(lambda peer: return_copy(peer).start())
    rbuf[mine, :] = obuf[mine, :]

    for stage in o_stages[1:]:
        stage()
    w_copies[3].wait()
    mixer_ref[...] = dot(hobuf[...], wout[...]).astype(BF16)

    loop(1, n_ep, lambda i: returned(lax.rem(ep + i, n_ep)).wait_recv())
    back = rbuf[...]
    weight = rw_ref[...]
    mix_ref[...] = (dot(picks[0], back) * weight[:, 0:1] + dot(picks[1], back) * weight[:, 1:2]).astype(BF16)

    for kv in range(2):
        for direction in range(2):
            if last[direction] >= 1:
                hop(direction, 1, kv, z).wait_send()
        handover(0, 0, kv, z).wait_send()

    def drain(s):
        for direction in range(2):

            @pl.when(s <= last[direction])
            def _(direction=direction):
                for kv in range(2):
                    owner = owner_of(direction, s)
                    handover(direction, s, kv, owner).wait_send()

                    @pl.when(s < last[direction])
                    def _(direction=direction, kv=kv, owner=owner):
                        hop(direction, s + 1, kv, owner).wait_send()

    loop(1, steps + 1, drain)
    loop(1, n_tp, lambda i: ss_copy(i).wait_send())
    others(lambda peer: dispatch_copy(peer).wait_send())
    others(lambda peer: return_copy(peer).wait_send())
    x_sent()
    h_sent()
    o_sent()


def per_device(nz, ny, nx, *args):
    q, k, v, scale, hgain, wout, x, ngain, ids, rw, gate, up, down = args
    ta, hd2 = q.shape
    vd = v.shape[1]
    tb, dcol = x.shape
    n_ep, n_tp = 2 * nz, ny * nx
    cap = 2 * tb * ids.shape[1] // n_ep
    slots = n_ep * cap
    d, ff = gate.shape[1:]
    gate, up, down = gate.reshape(d, ff), up.reshape(d, ff), down.reshape(down.shape[1:])
    ocol = down.shape[1]
    steps = nz // 2
    vmem = pl.BlockSpec(memory_space=pltpu.VMEM)
    hbm = pl.BlockSpec(memory_space=pl.ANY)
    dma = pltpu.SemaphoreType.DMA
    return pl.pallas_call(
        functools.partial(kernel, nz, ny, nx, cap),
        out_shape=(
            jax.ShapeDtypeStruct((ta, wout.shape[1]), BF16),
            jax.ShapeDtypeStruct((tb, ocol), BF16),
        ),
        in_specs=[
            vmem, vmem, vmem, pl.BlockSpec(memory_space=pltpu.SMEM), vmem, hbm, vmem, vmem, vmem, vmem, hbm, hbm, hbm,
        ],
        out_specs=(vmem, vmem),
        scratch_shapes=[
            pltpu.VMEM((n_ep, ta, hd2), BF16),
            pltpu.VMEM((nz, vd + 16, 2 * ta), BF16),
            pltpu.VMEM((2 * hd2, 2 * ta), BF16),
            pltpu.VMEM((1, 2 * ta), F32),
            pltpu.VMEM((vd + 16, 2 * ta), F32),
            pltpu.VMEM((n_tp, 8, tb), F32),
            pltpu.VMEM((slots, dcol), BF16),
            pltpu.VMEM((n_tp, slots, dcol), BF16),
            pltpu.VMEM((slots, 2 * ff), F32),
            pltpu.VMEM((slots, n_tp * ff), BF16),
            pltpu.VMEM((slots, ocol), BF16),
            pltpu.VMEM((slots, ocol), BF16),
            pltpu.VMEM((ta, n_tp * vd), BF16),
            pltpu.VMEM((2, tb, slots), BF16),
            pltpu.VMEM((d, 2 * ff), BF16),
            pltpu.VMEM(down.shape, BF16),
            pltpu.VMEM(wout.shape, BF16),
            dma((4,)),
            dma((1,)),
            dma((1,)),
            dma((2, steps + 1, 2)),
            dma((2, steps + 1, 2)),
            dma((2, steps + 1, 2)),
            dma((2, steps + 1, 2)),
            dma((n_tp,)),
            dma((n_tp,)),
            dma((2, n_ep)),
            dma((2, n_ep)),
            dma((3, 2, 20)),
            dma((3, 2, 20)),
        ],
        compiler_params=pltpu.CompilerParams(
            collective_id=0, has_side_effects=True, vmem_limit_bytes=60 * 1024 * 1024
        ),
        name="layer",
    )(q, k, v, scale, hgain.reshape(1, -1), wout, x, ngain.reshape(1, -1), ids, rw, gate, up, down)


def solution(mesh):
    placed = (
        P("ep", "tp"),
        P("ep", "tp"),
        P("ep", "tp"),
        P("tp"),
        P(),
        P(None, "tp"),
        P("ep", "tp"),
        P(),
        P("ep", None),
        P("ep", None),
        P("ep", None, "tp"),
        P("ep", None, "tp"),
        P("ep", None, "tp"),
    )
    ny, nx = PLANE[mesh.shape["tp"]]
    return jax.shard_map(
        functools.partial(per_device, mesh.shape["ep"] // 2, ny, nx),
        mesh=mesh,
        in_specs=placed,
        out_specs=(P("ep", "tp"), P("ep", "tp")),
        check_vma=False,
    )
```

time: 362 us -> 117 us (0.32)
  waiting for transfers between devices: 175 us -> 0 us
  Pallas kernels: 0 us -> 109 us
  matrix products: 77 us -> 0 us
  blocking collectives: 39 us -> 0 us
  other arithmetic: 21.3 us -> 0 us
  local copies, waits for them, and re-layouts: 25.7 us -> 4.44 us
  between operations: 14.7 us -> 1.3 us
  starting transfers between devices: 8.09 us -> 0 us
    all_gather x4 -> x0, waiting for transfers between devices: 153 us -> none  [the longest x1 73.7 us: side_by_side(): lax.all_gather(both, axis, axis=dim, tiled=True)]
    pallas_call x0 -> x1, Pallas kernels: none -> 109 us  [per_device(): pl.pallas_call(functools.partial(kernel, nz, ny, nx, cap), out_shape=(jax...]
    dot_general x28 -> x0, matrix products: 77 us -> none  [the longest x12 38.9 us: key_block(): jnp.einsum('ihcj,jhe->ihce', weights.astype(jnp.bfloat16), value_three, p...]
    all_to_all x1 -> x0, blocking collectives: 39 us -> none  [per_device(): lax.all_to_all(outgoing, 'ep', split_axis=0, concat_axis=0, tiled=True)]
    all_to_all x1 -> x0, waiting for transfers between devices: 22.1 us -> none  [per_device(): lax.all_to_all(moe_total.astype(jnp.bfloat16), 'ep', split_axis=0, concat...]
    reduce_sum x16 -> x0, other arithmetic: 14.6 us -> none  [the longest x12 10.2 us: key_block(): new_sum = old_sum * shrink + jnp.sum(weights, axis=-1)]
    dynamic_slice x12 -> x0, local copies, waits for them, and re-layouts: 11.7 us -> none  [step_block(): lax.dynamic_slice_in_dim(key_part, offset_rows, key_block_rows, 0)]
    all_to_all x1 -> x0, starting transfers between devices: 7.93 us -> none  [per_device(): lax.all_to_all(moe_total.astype(jnp.bfloat16), 'ep', split_axis=0, concat...]
  transfers between devices with their start and end apart: 5 -> 0, of which waited for: 4 -> 0; matrix products, arithmetic and copies ran while one was open for 31% -> 0% of each run, Pallas kernels for 0% -> 0%
where the time goes in v1:
time: 117 us; the launch traced here: 115 us
  Pallas kernels  109 us (93%)
  local copies, waits for them, and re-layouts  4.44 us (4%)
  between operations  1.3 us (1%)
    pallas_call x1, Pallas kernels, per_device(): pl.pallas_call(functools.partial(kernel, nz, ny, nx, cap), out_shape=(jax...  109 us
    unnamed x10, local copies, waits for them, and re-layouts  4.44 us

profile of v1, /device:TPU:1, one launch (start us, length us, event | category | flops | bytes accessed | tf_op | source)
XLA Modules:
  0.0 115.0 jit_solution(3577767731361464717)
XLA Ops:
  1.3 0.0 copy-start.1
  1.3 0.7 copy-done.1
  2.0 0.0 copy-start.2
  2.0 0.7 copy.15.ids_ref
  2.7 0.0 copy-done.2
  2.7 0.7 copy.16.rw_ref
  3.4 109.3 %layer.1 = (bf16[384,256]{1,0:T(8,128)(2,1)}, bf16[128,256]{1,0:T(8,128)(2,1)}) custom-call(bf16[384,128]{1,0:T(8,128)(2,1)} %q_ref.1, bf16[384,128]{1,0:T(8,128)(2,1)} %k_ref.1, bf16[384,128]{1,0:T(8,128)(2,1)} %v_ref.1, f32[1]{0:T(128)S(6)} %copy.19.scale_ref, f32[1,128]{1,0:T(1,128)} %bitcast.9, bf16[2048,256]{1,0:T(8,128)(2,1)} %wout_hbm.1, ...), custom_call_target="tpu_custom_call" | custom-call | tf_op jit(solution)/shard_map/layer/pallas_call | solution.py:580
  112.7 0.0 copy-start
  112.7 1.6 %copy.20 = bf16[384,256]{1,0:T(8,128)(2,1)} copy(bf16[384,256]{1,0:T(8,128)(2,1)} %get-tuple-element.4) | data formatting | bytes 393216
  114.4 0.0 copy-done
  114.4 0.6 copy.21
Async XLA Ops:
  1.3 0.7 copy-start.1
  2.0 0.7 copy-start.2
  112.7 1.7 %copy-start = (bf16[128,256]{1,0:T(8,128)(2,1)S(1)}, bf16[128,256]{1,0:T(8,128)(2,1)}, u32[]{:S(2)}) copy-start(bf16[128,256]{1,0:T(8,128)(2,1)} %get-tuple-element.5) | copy-start | bytes 196612

commit v2 on v1

v2 whole, which is shorter than its diff:
```python
import functools
import math

import jax
import jax.numpy as jnp
from jax import lax
from jax.experimental import pallas as pl
from jax.experimental.pallas import tpu as pltpu
from jax.sharding import PartitionSpec as P

MESH = pl.DeviceIdType.MESH
F32 = jnp.float32
BF16 = jnp.bfloat16
EPS = 1e-06
HEAD_FACTOR = 0.8
NEG = -1e30
PLANE = {16: (4, 4), 1: (1, 1)}
PLAN = (
    [("x", 0, 0), ("x", 1, 0)],
    {
        0: [("x", 0, 1)],
        1: [("x", 0, 30)],
        2: [("x", 1, 1)],
        3: [("x", 1, 30)],
        4: [("x", 0, 2)],
        5: [("x", 0, 31)],
        6: [("x", 0, 32)],
        7: [("x", 1, 2)],
        8: [("x", 1, 31)],
        9: [("x", 1, 32)],
        11: [("x", 0, 33)],
        12: [("sides", 0, 0)],
        14: [("x", 1, 33)],
        15: [("sides", 1, 0)],
        16: [("x", 0, 5), ("x", 1, 5)],
        18: [("h", 0, 1), ("h", 0, 30)],
        19: [("h", 1, 1), ("h", 1, 30)],
        21: [("h", 0, 2), ("h", 0, 31), ("h", 0, 32)],
        22: [("h", 1, 2)],
        23: [("h", 1, 31)],
        24: [("h", 1, 32)],
        25: [("h", 0, 33)],
        26: [("h", 1, 33)],
        28: [("h", 0, 5), ("h", 1, 5)],
    },
)


def dot(a, b):
    return lax.dot_general(a, b, (((1,), (0,)), ((), ())), preferred_element_type=F32)


def kernel(
    nz,
    ny,
    nx,
    cap,
    q_ref,
    k_ref,
    v_ref,
    scale_ref,
    hgain_ref,
    wout_hbm,
    x_ref,
    ngain_ref,
    ids_ref,
    rw_ref,
    gate_hbm,
    up_hbm,
    down_hbm,
    mixer_ref,
    mix_ref,
    kbuf,
    vbuf,
    qq,
    m_ref,
    acc,
    gs,
    ssq,
    disp,
    xbuf,
    gu,
    hbuf,
    obuf,
    rbuf,
    hobuf,
    picks,
    wgu,
    wdown,
    wout,
    w_sem,
    ring_send,
    ring_recv,
    pass_send,
    pass_recv,
    a2a_send,
    a2a_recv,
    xy_send,
    xy_recv,
):
    n_ep, n_tp = 2 * nz, ny * nx
    ta, hd2 = q_ref.shape
    vd = v_ref.shape[1]
    tb, dcol = x_ref.shape
    slots = n_ep * cap
    ff = gate_hbm.shape[1]
    ocol = wdown.shape[1]
    steps = nz // 2

    ep = lax.axis_index("ep")
    tp = lax.axis_index("tp")
    z, c = lax.div(ep, 2), lax.rem(ep, 2)
    y, x = lax.div(tp, nx), lax.rem(tp, nx)

    def at_ep(zz, cc):
        return {"ep": 2 * zz + cc}

    def remote(src, dst, ssem, rsem, dev):
        return pltpu.make_async_remote_copy(
            src_ref=src, dst_ref=dst, send_sem=ssem, recv_sem=rsem, device_id=dev, device_id_type=MESH
        )

    barrier = pltpu.get_barrier_semaphore()

    def greet_ep(i, carry):
        pl.semaphore_signal(barrier, inc=1, device_id={"ep": lax.rem(ep + i, n_ep)}, device_id_type=MESH)
        return carry

    def greet_tp(i, carry):
        pl.semaphore_signal(barrier, inc=1, device_id={"tp": lax.rem(tp + i, n_tp)}, device_id_type=MESH)
        return carry

    lax.fori_loop(1, n_ep, greet_ep, 0)
    if n_tp > 1:
        lax.fori_loop(1, n_tp, greet_tp, 0)

    w_copies = [
        pltpu.make_async_copy(gate_hbm, wgu.at[:, pl.ds(0, ff)], w_sem.at[0]),
        pltpu.make_async_copy(up_hbm, wgu.at[:, pl.ds(ff, ff)], w_sem.at[1]),
        pltpu.make_async_copy(down_hbm, wdown, w_sem.at[2]),
        pltpu.make_async_copy(wout_hbm, wout, w_sem.at[3]),
    ]
    for copy in w_copies:
        copy.start()

    v_t = v_ref[...].astype(F32).T.astype(BF16)

    @pl.when(c == 0)
    def _():
        vbuf[z, 0:vd, 0:ta] = v_t

    @pl.when(c == 1)
    def _():
        vbuf[z, 0:vd, ta : 2 * ta] = v_t

    kbuf[ep] = k_ref[...]

    def ones_rows(i, carry):
        vbuf[i, vd : vd + 16, :] = jnp.ones((16, 2 * ta), BF16)
        return carry

    lax.fori_loop(0, nz, ones_rows, 0)

    half = hd2 // 2
    q_t = (q_ref[...].astype(F32) * (math.log2(math.e) * half**-0.5)).T
    q_hi = q_t.astype(BF16)
    q_lo = (q_t - q_hi.astype(F32)).astype(BF16)
    none = jnp.zeros((half, ta), BF16)
    for i, part in enumerate((q_hi, q_lo)):
        qq[2 * half * i : 2 * half * i + half, 0:ta] = part[0:half]
        qq[2 * half * i : 2 * half * i + half, ta : 2 * ta] = none
        qq[2 * half * i + half : 2 * half * (i + 1), 0:ta] = none
        qq[2 * half * i + half : 2 * half * (i + 1), ta : 2 * ta] = part[half:]
    m_ref[...] = jnp.full(m_ref.shape, NEG, F32)
    acc[...] = jnp.zeros(acc.shape, F32)
    gu[...] = jnp.zeros(gu.shape, F32)
    ssq[...] = jnp.zeros(ssq.shape, F32)
    for i in range(gs.shape[0]):
        gs[i : i + 1, :] = ngain_ref[:, 128 * i : 128 * (i + 1)]

    def column(row):
        return jnp.broadcast_to(row, (128, tb)).T

    ids = [column(ids_ref[i : i + 1, :].astype(F32)) for i in range(2)]
    lane = lax.broadcasted_iota(jnp.int32, (tb, 128), 1).astype(F32)
    first = jnp.where(ids[0] == lane, 1.0, 0.0).astype(F32)
    second = jnp.where(ids[1] == lane, 1.0, 0.0).astype(F32)
    lower = jnp.where(
        lax.broadcasted_iota(jnp.int32, (tb, tb), 0) > lax.broadcasted_iota(jnp.int32, (tb, tb), 1), 1.0, 0.0
    ).astype(BF16)
    before_0 = dot(lower, first.astype(BF16))
    before_1 = dot(lower, second.astype(BF16)) + jnp.sum(first, axis=0, keepdims=True)
    rank_0 = jnp.sum(first * before_0, axis=1, keepdims=True)
    rank_1 = jnp.sum(second * before_1, axis=1, keepdims=True)
    slot_0 = ids[0][:, 0:1] * cap + rank_0
    slot_1 = ids[1][:, 0:1] * cap + rank_1
    slot_lane = lax.broadcasted_iota(jnp.int32, (tb, slots), 1).astype(F32)
    pick_0 = jnp.where(slot_0 == slot_lane, 1.0, 0.0).astype(F32)
    pick_1 = jnp.where(slot_1 == slot_lane, 1.0, 0.0).astype(F32)
    picks[0] = pick_0.astype(BF16)
    picks[1] = pick_1.astype(BF16)
    disp[...] = dot((pick_0 + pick_1).T.astype(BF16), x_ref[...]).astype(BF16)

    with jax.named_scope("barrier"):
        pl.semaphore_wait(barrier, (n_ep - 1) + (n_tp - 1))

    def loop(lo, hi, f):
        if not isinstance(lo, int) or not isinstance(hi, int) or hi > lo:
            lax.fori_loop(lo, hi, lambda i, carry: (f(i), carry)[1], 0)

    def chip_at(k):
        away = steps - lax.div(k + 1, 2)
        return lax.rem(jnp.where(lax.rem(k, 2) == 1, z + away, z - away + nz), nz)

    def mirrored(k):
        swapped = jnp.where(lax.rem(k, 2) == 1, k + 1, k - 1)
        return jnp.where(jnp.logical_or(k == 0, k == nz - 1), k, swapped)

    def rows_of(i):
        return pl.ds(pl.multiple_of(i * cap, cap), cap)

    def dispatch_copy(i):
        k, core = lax.div(i, 2), lax.rem(i, 2)
        peer = 2 * chip_at(k) + core
        there = 2 * mirrored(k) + c
        return remote(disp.at[rows_of(peer)], xbuf.at[tp, rows_of(there)], a2a_send.at[0, i], a2a_recv.at[0, there], {"ep": peer})

    def dispatched(i):
        peer = 2 * chip_at(lax.div(i, 2)) + lax.rem(i, 2)
        return remote(disp.at[rows_of(peer)], xbuf.at[tp, rows_of(i)], a2a_send.at[0, i], a2a_recv.at[0, i], {"ep": peer})

    def return_copy(i):
        peer = 2 * chip_at(lax.div(i, 2)) + lax.rem(i, 2)
        return remote(obuf.at[rows_of(i)], rbuf.at[rows_of(ep)], a2a_send.at[1, i], a2a_recv.at[1, ep], {"ep": peer})

    def returned(peer):
        return remote(obuf.at[rows_of(0)], rbuf.at[rows_of(peer)], a2a_send.at[1, 0], a2a_recv.at[1, peer], {"ep": peer})

    self_place = 2 * (nz - 1) + c

    def others(lo, hi, f):
        def each(i):
            pl.when(i != self_place)(lambda: f(i))

        loop(lo, hi, each)

    others(0, n_ep, lambda i: dispatch_copy(i).start())
    xbuf[tp, rows_of(self_place), :] = disp[rows_of(ep), :]

    def k_at(zz, cc):
        return kbuf.at[2 * zz + cc]

    def v_at(zz, cc):
        return vbuf.at[zz, pl.ds(0, vd), pl.ds(pl.multiple_of(cc * ta, 128), ta)]

    def part(owner, core, e):
        return (k_at, v_at)[e % 2](owner, core if e < 2 else 1 - core)

    last = jnp.where(c == 0, steps, nz - 1 - steps)
    next_chip = jnp.where(c == 0, lax.rem(z + 1, nz), lax.rem(z - 1 + nz, nz))

    def owner_of(core, s):
        return lax.rem(jnp.where(core == 0, z - s + nz, z + s), nz)

    def comes(core, s):
        low = nz - 2 - steps
        up, down = z - s >= 0, z + s - nz >= 0
        brought = jnp.where(core == 0, up & (s <= steps), (owner_of(core, s) <= low) & (s <= low + 1))
        return brought, brought & ((core == 0) | down)

    def goes(s):
        low = nz - 2 - steps
        return jnp.where(
            c == 0,
            (z + 1 < nz) & (z - (s - 1) >= 0) & (s <= steps),
            (owner_of(c, s - 1) <= low) & (s <= low + 1),
        )

    def hop(s, e):
        ref = part(owner_of(c, s - 1), c, e)
        return remote(ref, ref, ring_send.at[s, e], ring_recv.at[s, e], at_ep(next_chip, c))

    def hopped(s, e):
        ref = part(owner_of(c, s), c, e)
        return remote(ref, ref, ring_send.at[s, e], ring_recv.at[s, e], at_ep(next_chip, c))

    def handover(s, e):
        ref = part(owner_of(c, s), c, e)
        return remote(ref, ref, pass_send.at[s, e], pass_recv.at[s, e], at_ep(z, 1 - c))

    def handed(s, e):
        ref = part(owner_of(1 - c, s), 1 - c, e)
        return remote(ref, ref, pass_send.at[s, e], pass_recv.at[s, e], at_ep(z, 1 - c))

    for e in range(2):
        pl.when(goes(1))(lambda e=e: hop(1, e).start())
        handover(0, e).start()

    def ring_event(s, e):
        brought, used = comes(c, s)

        @pl.when(brought)
        def _():
            hopped(s, e).wait_recv()
            pl.when(goes(s + 1))(lambda: hop(s + 1, e).start())
            pl.when(used)(lambda: handover(s, e).start())

    n_tile = 256 if (2 * ta) % 256 == 0 else 2 * ta
    tiles = 2 * ta // n_tile

    def attend(owner, n, masked):
        cols = pl.ds(pl.multiple_of(n * n_tile, n_tile), n_tile)
        keys = kbuf[pl.ds(2 * owner, 2)].reshape(2 * ta, hd2)
        keys = jnp.concatenate([keys, keys], axis=1)
        s = dot(keys, qq[:, cols])
        if masked:
            row = lax.broadcasted_iota(jnp.int32, s.shape, 0)
            col = lax.broadcasted_iota(jnp.int32, s.shape, 1) + n * n_tile
            col = jnp.where(col >= ta, col - ta, col) + c * ta
            s = jnp.where(row <= col, s, NEG)
        old = m_ref[:, cols]
        new = jnp.maximum(old, jnp.max(s, axis=0, keepdims=True))
        weights = jnp.exp2(s - new).astype(BF16)
        shrink = jnp.exp2(old - new)
        m_ref[:, cols] = new
        acc[:, cols] = acc[:, cols] * shrink + dot(vbuf[owner], weights)

    with jax.named_scope("own_wait"):
        for e in range(2):
            handed(0, e).wait_recv()
            pl.when(goes(1))(lambda e=e: hop(1, 2 + e).start())
    with jax.named_scope("own_attend"):
        loop(0, tiles, lambda n: attend(z, n, True))

    with jax.named_scope("gain"):
        w_copies[0].wait()
        w_copies[1].wait()
        gain = gs[...].T
        for i in range(gs.shape[0]):
            rows = slice(128 * i, 128 * (i + 1))
            wgu[rows, :] = (wgu[rows, :].astype(F32) * gain[:, i : i + 1]).astype(BF16)

    def plane_gather(number, rows, block):
        quarter = rows // 2

        def half_stages(h):
            size_p, size_s = (nx, ny) if h == 0 else (ny, nx)
            p, s = (x, y) if h == 0 else (y, x)

            def index(ss, pp):
                ss, pp = lax.rem(ss + 4, 4), lax.rem(pp + 4, 4)
                return ss * nx + pp if h == 0 else pp * nx + ss

            rel = (0, -1, 1, 2)
            whole, low, high = (0, rows), (0, quarter), (quarter, quarter)

            def msg(name, ds, dp, part):
                sem = {"pr": 0, "pl": 1, "fr": 2, "fl": 3}.get(name)
                if sem is None:
                    sem = 4 + 4 * ("su", "sd", "gu", "gd").index(name[:2]) + int(name[2])
                ts, tp_ = {
                    "pr": (0, 1), "pl": (0, -1), "fr": (0, 1), "fl": (0, -1),
                    "su": (1, 0), "sd": (-1, 0), "gu": (1, 0), "gd": (-1, 0),
                }[name if sem < 4 else name[:2]]
                ref = block(h, index(s + ds, p + dp), *part)
                return remote(
                    ref, ref, xy_send.at[number, h, sem], xy_recv.at[number, h, sem], {"tp": index(s + ts, p + tp_)}
                )

            sent = []

            def send(name, ds, dp, part):
                msg(name, ds, dp, part).start()
                sent.append(lambda: msg(name, ds, dp, part).wait_send())

            def prime():
                send("pr", 0, 0, whole)
                send("pl", 0, 0, whole)

            def out(j):
                send(f"su{j}", 0, rel[j], whole)
                send(f"sd{j}", 0, rel[j], whole)

            def across():
                msg("pr", 0, -1, whole).wait_recv()
                send("fr", 0, -1, low)
                msg("pl", 0, 1, whole).wait_recv()
                send("fl", 0, 1, high)

            def opposite():
                msg("fr", 0, -2, low).wait_recv()
                msg("fl", 0, 2, high).wait_recv()

            def forward(j):
                msg(f"su{j}", -1, rel[j], whole).wait_recv()
                send(f"gu{j}", -1, rel[j], low)
                msg(f"sd{j}", 1, rel[j], whole).wait_recv()
                send(f"gd{j}", 1, rel[j], high)

            def ended(j):
                msg(f"gu{j}", -2, rel[j], low).wait_recv()
                msg(f"gd{j}", 2, rel[j], high).wait_recv()

            steps_of = {
                0: [prime, lambda: out(0)],
                1: [across, lambda: (out(1), out(2))],
                2: [opposite, lambda: out(3)],
                5: [lambda: [ended(j) for j in range(4)]],
            }
            for j in range(4):
                steps_of[30 + j] = [functools.partial(forward, j)]
            return steps_of, sent

        if n_tp == 1:
            return lambda i: None, lambda: None
        (a, sent_a), (b, sent_b) = half_stages(0), half_stages(1)

        def both(i):
            with jax.named_scope(f"g{number}_{i}"):
                for one, two in zip(a[i], b[i]):
                    one()
                    two()

        def drained():
            for wait in sent_a + sent_b:
                wait()

        return both, drained

    passes = 2
    rows_p = slots // passes
    rows_x = rows_p // 2

    def x_block(p, h, owner, row, count):
        return xbuf.at[owner, pl.ds(p * rows_p + h * rows_x + row, count)]

    def h_block(p, h, owner, row, count):
        return hbuf.at[pl.ds(p * rows_p + h * rows_x + row, count), pl.ds(pl.multiple_of(owner * ff, 128), ff)]

    rows_a = ta // 2

    def ho_block(h, owner, row, count):
        return hobuf.at[pl.ds(h * rows_a + row, count), pl.ds(pl.multiple_of(owner * vd, 128), vd)]

    xs = [plane_gather(p, rows_x, functools.partial(x_block, p)) for p in range(passes)]
    hs = [plane_gather(passes + p, rows_x, functools.partial(h_block, p)) for p in range(passes)]
    o_stage, o_sent = plane_gather(2 * passes, rows_a, ho_block)

    def add_group(p, h, ds):
        at = slice(p * rows_p + h * rows_x, p * rows_p + (h + 1) * rows_x)
        if n_tp == 1:
            owners = [0]
        elif h == 0:
            owners = [lax.rem(y + ds + ny, ny) * nx + j for j in range(nx)]
        else:
            owners = [j * nx + lax.rem(x + ds + nx, nx) for j in range(ny)]
        total, squares = gu[at, :], ssq[at, :]
        for owner in owners:
            rows = xbuf[owner, at, :]
            total = total + dot(rows, wgu[pl.ds(pl.multiple_of(owner * dcol, dcol), dcol), :])
            wide = rows.astype(F32)
            wide = wide * wide
            for j in range(dcol // 128):
                squares = squares + wide[:, 128 * j : 128 * (j + 1)]
        gu[at, :] = total
        ssq[at, :] = squares

    def x_stage(p, i):
        if i == 0:
            with jax.named_scope("disp_wait"):
                others(2 * nz // passes * p, 2 * nz // passes * (p + 1), lambda j: dispatched(j).wait_recv())
        xs[p][0](i)
        with jax.named_scope("gate_up"):
            for ds in {32: (0,), 5: (2,)}.get(i, ()) if n_tp > 1 else (0,) * (i == 5):
                for h in range(2):
                    add_group(p, h, ds)
        if i == 5:
            at = slice(p * rows_p, (p + 1) * rows_p)
            mean = jnp.sum(ssq[at, :], axis=1, keepdims=True) / (n_tp * dcol)
            both = gu[at, :] * lax.rsqrt(mean + EPS)
            gate, up = both[:, 0:ff], both[:, ff : 2 * ff]
            hidden = (gate / (1.0 + jnp.exp(-gate)) * up).astype(BF16)
            hbuf[at, pl.ds(pl.multiple_of(tp * ff, 128), ff)] = hidden
            hs[p][0](0)

    def h_stage(p, i):
        hs[p][0](i)
        if i == 5:
            at = slice(p * rows_p, (p + 1) * rows_p)
            if p == 0:
                w_copies[2].wait()
            with jax.named_scope("down"):
                obuf[at, :] = dot(hbuf[at, :], wdown[...]).astype(BF16)
            others(2 * nz // passes * p, 2 * nz // passes * (p + 1), lambda j: return_copy(j).start())
            if p == passes - 1:
                rbuf[rows_of(ep), :] = obuf[rows_of(self_place), :]

    def run(items):
        for what, p, i in items:
            if what == "sides":
                if n_tp > 1:
                    with jax.named_scope("gate_up"):
                        for ds in (-1, 1):
                            for h in range(2):
                                add_group(p, h, ds)
            else:
                (x_stage if what == "x" else h_stage)(p, i)

    def use(core, s, lo, hi):
        _, used = comes(core, s)

        @pl.when(used & (s >= 1))
        def _():
            if lo == 0:

                @pl.when(c != core)
                def _():
                    with jax.named_scope("handed"):
                        for e in range(4):
                            handed(s, e).wait_recv()

            with jax.named_scope("attend"):
                loop(lo, hi, lambda n: attend(owner_of(core, s), n, False))

    run(PLAN[0])
    split = tiles - tiles // 3

    def tick(s):
        for e in range(4):
            with jax.named_scope("ring"):
                ring_event(s, e)
            for at, items in PLAN[1].items():
                if at % 4 == e and at // 4 + 1 <= steps + 1:
                    pl.when(s == at // 4 + 1)(functools.partial(run, items))
            use(e // 2, s - 1, *((0, split), (split, tiles))[e % 2])

    loop(1, steps + 2, tick)
    for at, items in PLAN[1].items():
        if at // 4 + 1 > steps + 1:
            run(items)

    def sent_so_far():
        for e in range(2):
            handover(0, e).wait_send()

        def drain(s):
            _, used = comes(c, s)
            for e in range(4):
                pl.when(goes(s))(lambda e=e: hop(s, e).wait_send())
                pl.when(used)(lambda e=e: handover(s, e).wait_send())

        loop(1, steps + 1, drain)
        others(0, n_ep, lambda i: dispatch_copy(i).wait_send())
        for _, sent in xs + hs:
            sent()

    maps = acc[0:vd, :] / acc[vd : vd + 1, :]
    mixed = maps[:, 0:ta] - scale_ref[0] * maps[:, ta : 2 * ta]
    mean_sq = jnp.mean(mixed * mixed, axis=0, keepdims=True)
    head = (mixed * lax.rsqrt(mean_sq + EPS)).T * hgain_ref[...] * HEAD_FACTOR
    hobuf[:, pl.ds(pl.multiple_of(tp * vd, 128), vd)] = head.astype(BF16)
    o_stage(0)

    sent_so_far()
    for i in (1, 30, 2, 31, 32, 33, 5):
        o_stage(i)
    w_copies[3].wait()
    with jax.named_scope("outproj"):
        mixer_ref[...] = dot(hobuf[...], wout[...]).astype(BF16)

    def other_experts(f):
        loop(1, n_ep, lambda i: f(lax.rem(ep + i, n_ep)))

    with jax.named_scope("ret_wait"):
        other_experts(lambda peer: returned(peer).wait_recv())
    back = rbuf[...]
    weight = [column(rw_ref[i : i + 1, :])[:, 0:1] for i in range(2)]
    mix_ref[...] = (dot(picks[0], back) * weight[0] + dot(picks[1], back) * weight[1]).astype(BF16)

    others(0, n_ep, lambda i: return_copy(i).wait_send())
    o_sent()


def per_device(nz, ny, nx, *args):
    q, k, v, scale, hgain, wout, x, ngain, ids, rw, gate, up, down = args
    ta, hd2 = q.shape
    vd = v.shape[1]
    tb, dcol = x.shape
    n_ep, n_tp = 2 * nz, ny * nx
    cap = 2 * tb * ids.shape[1] // n_ep
    slots = n_ep * cap
    d, ff = gate.shape[1:]
    gate, up, down = gate.reshape(d, ff), up.reshape(d, ff), down.reshape(down.shape[1:])
    ocol = down.shape[1]
    steps = nz // 2
    vmem = pl.BlockSpec(memory_space=pltpu.VMEM)
    hbm = pl.BlockSpec(memory_space=pl.ANY)
    dma = pltpu.SemaphoreType.DMA
    return pl.pallas_call(
        functools.partial(kernel, nz, ny, nx, cap),
        out_shape=(
            jax.ShapeDtypeStruct((ta, wout.shape[1]), BF16),
            jax.ShapeDtypeStruct((tb, ocol), BF16),
        ),
        in_specs=[
            vmem, vmem, vmem, pl.BlockSpec(memory_space=pltpu.SMEM), vmem, hbm, vmem, vmem, vmem, vmem, hbm, hbm, hbm,
        ],
        out_specs=(vmem, vmem),
        scratch_shapes=[
            pltpu.VMEM((n_ep, ta, hd2), BF16),
            pltpu.VMEM((nz, vd + 16, 2 * ta), BF16),
            pltpu.VMEM((2 * hd2, 2 * ta), BF16),
            pltpu.VMEM((1, 2 * ta), F32),
            pltpu.VMEM((vd + 16, 2 * ta), F32),
            pltpu.VMEM((d // 128, 128), F32),
            pltpu.VMEM((slots, 128), F32),
            pltpu.VMEM((slots, dcol), BF16),
            pltpu.VMEM((n_tp, slots, dcol), BF16),
            pltpu.VMEM((slots, 2 * ff), F32),
            pltpu.VMEM((slots, n_tp * ff), BF16),
            pltpu.VMEM((slots, ocol), BF16),
            pltpu.VMEM((slots, ocol), BF16),
            pltpu.VMEM((ta, n_tp * vd), BF16),
            pltpu.VMEM((2, tb, slots), BF16),
            pltpu.VMEM((d, 2 * ff), BF16),
            pltpu.VMEM(down.shape, BF16),
            pltpu.VMEM(wout.shape, BF16),
            dma((4,)),
            dma((steps + 1, 4)),
            dma((steps + 1, 4)),
            dma((steps + 1, 4)),
            dma((steps + 1, 4)),
            dma((2, n_ep)),
            dma((2, n_ep)),
            dma((5, 2, 20)),
            dma((5, 2, 20)),
        ],
        compiler_params=pltpu.CompilerParams(
            collective_id=0, has_side_effects=True, vmem_limit_bytes=60 * 1024 * 1024
        ),
        name="layer",
    )(q, k, v, scale, hgain.reshape(1, -1), wout, x, ngain.reshape(1, -1), ids.T, rw.T, gate, up, down)


def solution(mesh):
    placed = (
        P("ep", "tp"),
        P("ep", "tp"),
        P("ep", "tp"),
        P("tp"),
        P(),
        P(None, "tp"),
        P("ep", "tp"),
        P(),
        P("ep", None),
        P("ep", None),
        P("ep", None, "tp"),
        P("ep", None, "tp"),
        P("ep", None, "tp"),
    )
    ny, nx = PLANE[mesh.shape["tp"]]
    return jax.shard_map(
        functools.partial(per_device, mesh.shape["ep"] // 2, ny, nx),
        mesh=mesh,
        in_specs=placed,
        out_specs=(P("ep", "tp"), P("ep", "tp")),
        check_vma=False,
    )
```

time: 117 us -> 104 us (0.89)
  the two profiles are of different devices: /device:TPU:1 before, /device:TPU:480 now
where the time goes in v2:
time: 104 us
  Pallas kernels  100 us (96%)
  local copies, waits for them, and re-layouts  2.28 us (2%)
  between operations  1.3 us (1%)
    pallas_call x1, Pallas kernels, per_device(): pl.pallas_call(functools.partial(kernel, nz, ny, nx, cap), out_shape=(jax...  100 us
    unnamed x4, local copies, waits for them, and re-layouts  2.28 us

profile of v2, /device:TPU:480, one launch (start us, length us, event | category | flops | bytes accessed | tf_op | source)
XLA Modules:
  0.0 104.0 jit_solution(16900800733574478358)
XLA Ops:
  1.3 100.4 %layer.1 = (bf16[384,256]{1,0:T(8,128)(2,1)}, bf16[128,256]{1,0:T(8,128)(2,1)}) custom-call(bf16[384,128]{1,0:T(8,128)(2,1)} %q_ref.1, bf16[384,128]{1,0:T(8,128)(2,1)} %k_ref.1, bf16[384,128]{1,0:T(8,128)(2,1)} %v_ref.1, f32[1]{0:T(128)S(6)} %copy.17.scale_ref, f32[1,128]{1,0:T(1,128)} %bitcast.13, bf16[2048,256]{1,0:T(8,128)(2,1)} %wout_hbm.1, ...), custom_call_target="tpu_custom_call" | custom-call | tf_op jit(solution)/shard_map/layer/pallas_call | solution.py:599
  101.7 0.0 copy-start
  101.7 1.6 %copy.18 = bf16[384,256]{1,0:T(8,128)(2,1)} copy(bf16[384,256]{1,0:T(8,128)(2,1)} %get-tuple-element.4) | data formatting | bytes 393216
  103.4 0.0 copy-done
  103.4 0.6 copy.19
Async XLA Ops:
  101.7 1.7 %copy-start = (bf16[128,256]{1,0:T(8,128)(2,1)S(1)}, bf16[128,256]{1,0:T(8,128)(2,1)}, u32[]{:S(2)}) copy-start(bf16[128,256]{1,0:T(8,128)(2,1)} %get-tuple-element.5) | copy-start | bytes 196612

commit v3 on v2

--- a/solution.py
+++ b/solution.py
@@ -16,33 +16,32 @@
 NEG = -1e30
 PLANE = {16: (4, 4), 1: (1, 1)}
 PLAN = (
-    [("x", 0, 0), ("x", 1, 0)],
+    [("x", 0, 0), ("x", 0, 10), ("x", 1, 0)],
     {
-        0: [("x", 0, 1)],
-        1: [("x", 0, 30)],
-        2: [("x", 1, 1)],
-        3: [("x", 1, 30)],
-        4: [("x", 0, 2)],
-        5: [("x", 0, 31)],
-        6: [("x", 0, 32)],
-        7: [("x", 1, 2)],
-        8: [("x", 1, 31)],
-        9: [("x", 1, 32)],
-        11: [("x", 0, 33)],
-        12: [("sides", 0, 0)],
-        14: [("x", 1, 33)],
-        15: [("sides", 1, 0)],
-        16: [("x", 0, 5), ("x", 1, 5)],
-        18: [("h", 0, 1), ("h", 0, 30)],
-        19: [("h", 1, 1), ("h", 1, 30)],
-        21: [("h", 0, 2), ("h", 0, 31), ("h", 0, 32)],
-        22: [("h", 1, 2)],
-        23: [("h", 1, 31)],
-        24: [("h", 1, 32)],
+        2: [("x", 0, 1), ("x", 0, 11)],
+        3: [("x", 0, 30)],
+        5: [("x", 1, 1), ("x", 0, 12), ("x", 0, 2)],
+        6: [("x", 1, 11), ("x", 1, 10)],
+        9: [("x", 0, 32)],
+        11: [("x", 0, 33), ("x", 0, 31), ("sides", 0, 0), ("x", 1, 2), ("x", 1, 12)],
+        13: [("x", 1, 30)],
+        15: [("x", 0, 5)],
+        17: [("x", 1, 33), ("x", 1, 31)],
+        18: [("x", 1, 32), ("sides", 1, 0)],
+        19: [("h", 0, 1)],
+        20: [("h", 0, 11), ("h", 0, 10), ("h", 0, 12)],
+        21: [("x", 1, 5)],
+        22: [("h", 0, 2)],
+        23: [("h", 0, 30)],
+        24: [("h", 0, 31), ("h", 0, 32)],
         25: [("h", 0, 33)],
-        26: [("h", 1, 33)],
-        28: [("h", 0, 5), ("h", 1, 5)],
+        26: [("h", 1, 1), ("h", 1, 12), ("h", 1, 10), ("h", 1, 11)],
+        28: [("h", 0, 5)],
+        29: [("h", 1, 2)],
+        30: [("h", 1, 30), ("h", 1, 31)],
+        31: [("h", 1, 32), ("h", 1, 33)],
     },
+    [("o", 0, 0), ("o", 0, 10), ("h", 1, 5), ("o", 0, 1), ("o", 0, 12), ("o", 0, 11), ("o", 0, 2), ("o", 0, 32), ("o", 0, 30), ("o", 0, 31), ("o", 0, 33), ("o", 0, 5)],
 )
 
 
@@ -208,6 +207,8 @@
         if not isinstance(lo, int) or not isinstance(hi, int) or hi > lo:
             lax.fori_loop(lo, hi, lambda i, carry: (f(i), carry)[1], 0)
 
+    passes = 2
+
     def chip_at(k):
         away = steps - lax.div(k + 1, 2)
         return lax.rem(jnp.where(lax.rem(k, 2) == 1, z + away, z - away + nz), nz)
@@ -223,18 +224,24 @@
         k, core = lax.div(i, 2), lax.rem(i, 2)
         peer = 2 * chip_at(k) + core
         there = 2 * mirrored(k) + c
-        return remote(disp.at[rows_of(peer)], xbuf.at[tp, rows_of(there)], a2a_send.at[0, i], a2a_recv.at[0, there], {"ep": peer})
-
-    def dispatched(i):
-        peer = 2 * chip_at(lax.div(i, 2)) + lax.rem(i, 2)
-        return remote(disp.at[rows_of(peer)], xbuf.at[tp, rows_of(i)], a2a_send.at[0, i], a2a_recv.at[0, i], {"ep": peer})
+        group = lax.div(there, n_ep // passes)
+        return remote(disp.at[rows_of(peer)], xbuf.at[tp, rows_of(there)], a2a_send.at[0], a2a_recv.at[group], {"ep": peer})
+
+    def wait_for(ref, sem):
+        pltpu.make_async_copy(ref, ref, sem).wait()
+
+    def dispatched(p):
+        each = n_ep // passes
+        if nz == 1:
+            pl.when(c != p)(lambda: wait_for(xbuf.at[0, pl.ds(0, cap)], a2a_recv.at[p]))
+        else:
+            wait_for(xbuf.at[0, pl.ds(0, (each - (p == passes - 1)) * cap)], a2a_recv.at[p])
 
     def return_copy(i):
         peer = 2 * chip_at(lax.div(i, 2)) + lax.rem(i, 2)
-        return remote(obuf.at[rows_of(i)], rbuf.at[rows_of(ep)], a2a_send.at[1, i], a2a_recv.at[1, ep], {"ep": peer})
-
-    def returned(peer):
-        return remote(obuf.at[rows_of(0)], rbuf.at[rows_of(peer)], a2a_send.at[1, 0], a2a_recv.at[1, peer], {"ep": peer})
+        return remote(obuf.at[rows_of(i)], rbuf.at[rows_of(ep)], a2a_send.at[1], a2a_recv.at[passes], {"ep": peer})
+
+    all_but_one = pl.ds(0, (n_ep - 1) * cap)
 
     self_place = 2 * (nz - 1) + c
 
@@ -278,19 +285,18 @@
 
     def hop(s, e):
         ref = part(owner_of(c, s - 1), c, e)
-        return remote(ref, ref, ring_send.at[s, e], ring_recv.at[s, e], at_ep(next_chip, c))
+        return remote(ref, ref, ring_send.at[s], ring_recv.at[s, e], at_ep(next_chip, c))
 
     def hopped(s, e):
         ref = part(owner_of(c, s), c, e)
-        return remote(ref, ref, ring_send.at[s, e], ring_recv.at[s, e], at_ep(next_chip, c))
+        return remote(ref, ref, ring_send.at[s], ring_recv.at[s, e], at_ep(next_chip, c))
 
     def handover(s, e):
         ref = part(owner_of(c, s), c, e)
-        return remote(ref, ref, pass_send.at[s, e], pass_recv.at[s, e], at_ep(z, 1 - c))
-
-    def handed(s, e):
-        ref = part(owner_of(1 - c, s), 1 - c, e)
-        return remote(ref, ref, pass_send.at[s, e], pass_recv.at[s, e], at_ep(z, 1 - c))
+        return remote(ref, ref, pass_send.at[s], pass_recv.at[s], at_ep(z, 1 - c))
+
+    def chunks(n):
+        return kbuf.at[pl.ds(0, min(n, n_ep))]
 
     for e in range(2):
         pl.when(goes(1))(lambda e=e: hop(1, e).start())
@@ -308,29 +314,36 @@
     n_tile = 256 if (2 * ta) % 256 == 0 else 2 * ta
     tiles = 2 * ta // n_tile
 
-    def attend(owner, n, masked):
-        cols = pl.ds(pl.multiple_of(n * n_tile, n_tile), n_tile)
+    def attend(owner, masked):
         keys = kbuf[pl.ds(2 * owner, 2)].reshape(2 * ta, hd2)
         keys = jnp.concatenate([keys, keys], axis=1)
-        s = dot(keys, qq[:, cols])
-        if masked:
-            row = lax.broadcasted_iota(jnp.int32, s.shape, 0)
-            col = lax.broadcasted_iota(jnp.int32, s.shape, 1) + n * n_tile
-            col = jnp.where(col >= ta, col - ta, col) + c * ta
-            s = jnp.where(row <= col, s, NEG)
-        old = m_ref[:, cols]
-        new = jnp.maximum(old, jnp.max(s, axis=0, keepdims=True))
-        weights = jnp.exp2(s - new).astype(BF16)
-        shrink = jnp.exp2(old - new)
-        m_ref[:, cols] = new
-        acc[:, cols] = acc[:, cols] * shrink + dot(vbuf[owner], weights)
+
+        def scores(n):
+            return dot(keys, qq[:, n * n_tile : (n + 1) * n_tile])
+
+        ahead = scores(0)
+        for n in range(tiles):
+            s, cols = ahead, slice(n * n_tile, (n + 1) * n_tile)
+            if n + 1 < tiles:
+                ahead = scores(n + 1)
+            if masked:
+                row = lax.broadcasted_iota(jnp.int32, s.shape, 0)
+                col = lax.broadcasted_iota(jnp.int32, s.shape, 1) + n * n_tile
+                col = jnp.where(col >= ta, col - ta, col) + c * ta
+                s = jnp.where(row <= col, s, NEG)
+            old = m_ref[:, cols]
+            new = jnp.maximum(old, jnp.max(s, axis=0, keepdims=True))
+            weights = jnp.exp2(s - new).astype(BF16)
+            shrink = jnp.exp2(old - new)
+            m_ref[:, cols] = new
+            acc[:, cols] = acc[:, cols] * shrink + dot(vbuf[owner], weights)
 
     with jax.named_scope("own_wait"):
-        for e in range(2):
-            handed(0, e).wait_recv()
-            pl.when(goes(1))(lambda e=e: hop(1, 2 + e).start())
+        wait_for(chunks(2), pass_recv.at[0])
+        for e in range(2, 4):
+            pl.when(goes(1))(lambda e=e: hop(1, e).start())
     with jax.named_scope("own_attend"):
-        loop(0, tiles, lambda n: attend(z, n, True))
+        attend(z, True)
 
     with jax.named_scope("gain"):
         w_copies[0].wait()
@@ -340,7 +353,7 @@
             rows = slice(128 * i, 128 * (i + 1))
             wgu[rows, :] = (wgu[rows, :].astype(F32) * gain[:, i : i + 1]).astype(BF16)
 
-    def plane_gather(number, rows, block):
+    def plane_gather(number, rows, block, span):
         quarter = rows // 2
 
         def half_stages(h):
@@ -354,24 +367,13 @@
             rel = (0, -1, 1, 2)
             whole, low, high = (0, rows), (0, quarter), (quarter, quarter)
 
-            def msg(name, ds, dp, part):
-                sem = {"pr": 0, "pl": 1, "fr": 2, "fl": 3}.get(name)
-                if sem is None:
-                    sem = 4 + 4 * ("su", "sd", "gu", "gd").index(name[:2]) + int(name[2])
-                ts, tp_ = {
-                    "pr": (0, 1), "pl": (0, -1), "fr": (0, 1), "fl": (0, -1),
-                    "su": (1, 0), "sd": (-1, 0), "gu": (1, 0), "gd": (-1, 0),
-                }[name if sem < 4 else name[:2]]
+            def send(name, ds, dp, part):
+                group = {"p": 0, "f": 1, "s": 2, "g": 6}[name[0]] + (int(name[2]) if name[0] == "s" else 0)
+                ts, tp_ = {"r": (0, 1), "l": (0, -1), "u": (1, 0), "d": (-1, 0)}[name[1]]
                 ref = block(h, index(s + ds, p + dp), *part)
-                return remote(
-                    ref, ref, xy_send.at[number, h, sem], xy_recv.at[number, h, sem], {"tp": index(s + ts, p + tp_)}
-                )
-
-            sent = []
-
-            def send(name, ds, dp, part):
-                msg(name, ds, dp, part).start()
-                sent.append(lambda: msg(name, ds, dp, part).wait_send())
+                remote(
+                    ref, ref, xy_send.at[number], xy_recv.at[number, group], {"tp": index(s + ts, p + tp_)}
+                ).start()
 
             def prime():
                 send("pr", 0, 0, whole)
@@ -382,52 +384,37 @@
                 send(f"sd{j}", 0, rel[j], whole)
 
             def across():
-                msg("pr", 0, -1, whole).wait_recv()
                 send("fr", 0, -1, low)
-                msg("pl", 0, 1, whole).wait_recv()
                 send("fl", 0, 1, high)
 
-            def opposite():
-                msg("fr", 0, -2, low).wait_recv()
-                msg("fl", 0, 2, high).wait_recv()
-
             def forward(j):
-                msg(f"su{j}", -1, rel[j], whole).wait_recv()
-                send(f"gu{j}", -1, rel[j], low)
-                msg(f"sd{j}", 1, rel[j], whole).wait_recv()
-                send(f"gd{j}", 1, rel[j], high)
-
-            def ended(j):
-                msg(f"gu{j}", -2, rel[j], low).wait_recv()
-                msg(f"gd{j}", 2, rel[j], high).wait_recv()
-
-            steps_of = {
-                0: [prime, lambda: out(0)],
-                1: [across, lambda: (out(1), out(2))],
-                2: [opposite, lambda: out(3)],
-                5: [lambda: [ended(j) for j in range(4)]],
-            }
+                send("gu", -1, rel[j], low)
+                send("gd", 1, rel[j], high)
+
+            sends = {0: prime, 10: lambda: out(0), 1: across, 11: lambda: out(1), 12: lambda: out(2), 2: lambda: out(3)}
             for j in range(4):
-                steps_of[30 + j] = [functools.partial(forward, j)]
-            return steps_of, sent
+                sends[30 + j] = functools.partial(forward, j)
+            return sends
 
         if n_tp == 1:
             return lambda i: None, lambda: None
-        (a, sent_a), (b, sent_b) = half_stages(0), half_stages(1)
+        first, second = half_stages(0), half_stages(1)
+        waits = {1: (0, 4), 2: (1, 2), 30: (2, 4), 31: (3, 4), 32: (4, 4), 33: (5, 4), 5: (6, 8)}
 
         def both(i):
             with jax.named_scope(f"g{number}_{i}"):
-                for one, two in zip(a[i], b[i]):
-                    one()
-                    two()
+                if i in waits:
+                    kind, count = waits[i]
+                    wait_for(span(count), xy_recv.at[number, kind])
+                if i in first:
+                    first[i]()
+                    second[i]()
 
         def drained():
-            for wait in sent_a + sent_b:
-                wait()
+            wait_for(span(30), xy_send.at[number])
 
         return both, drained
 
-    passes = 2
     rows_p = slots // passes
     rows_x = rows_p // 2
 
@@ -442,9 +429,18 @@
     def ho_block(h, owner, row, count):
         return hobuf.at[pl.ds(h * rows_a + row, count), pl.ds(pl.multiple_of(owner * vd, 128), vd)]
 
-    xs = [plane_gather(p, rows_x, functools.partial(x_block, p)) for p in range(passes)]
-    hs = [plane_gather(passes + p, rows_x, functools.partial(h_block, p)) for p in range(passes)]
-    o_stage, o_sent = plane_gather(2 * passes, rows_a, ho_block)
+    def x_span(n):
+        return xbuf.at[pl.ds(0, n // 2), pl.ds(0, 2 * rows_x)]
+
+    def h_span(n):
+        return hbuf.at[pl.ds(0, 2 * rows_x), pl.ds(0, n // 2 * ff)]
+
+    def ho_span(n):
+        return hobuf.at[pl.ds(0, 2 * rows_a), pl.ds(0, n // 2 * vd)]
+
+    xs = [plane_gather(p, rows_x, functools.partial(x_block, p), x_span) for p in range(passes)]
+    hs = [plane_gather(passes + p, rows_x, functools.partial(h_block, p), h_span) for p in range(passes)]
+    o_stage, o_sent = plane_gather(2 * passes, rows_a, ho_block, ho_span)
 
     def add_group(p, h, ds):
         at = slice(p * rows_p + h * rows_x, p * rows_p + (h + 1) * rows_x)
@@ -468,7 +464,7 @@
     def x_stage(p, i):
         if i == 0:
             with jax.named_scope("disp_wait"):
-                others(2 * nz // passes * p, 2 * nz // passes * (p + 1), lambda j: dispatched(j).wait_recv())
+                dispatched(p)
         xs[p][0](i)
         with jax.named_scope("gate_up"):
             for ds in {32: (0,), 5: (2,)}.get(i, ()) if n_tp > 1 else (0,) * (i == 5):
@@ -506,24 +502,20 @@
             else:
                 (x_stage if what == "x" else h_stage)(p, i)
 
-    def use(core, s, lo, hi):
+    def use(core, s):
         _, used = comes(core, s)
 
         @pl.when(used & (s >= 1))
         def _():
-            if lo == 0:
-
-                @pl.when(c != core)
-                def _():
-                    with jax.named_scope("handed"):
-                        for e in range(4):
-                            handed(s, e).wait_recv()
+            @pl.when(c != core)
+            def _():
+                with jax.named_scope("handed"):
+                    wait_for(chunks(4), pass_recv.at[s])
 
             with jax.named_scope("attend"):
-                loop(lo, hi, lambda n: attend(owner_of(core, s), n, False))
+                attend(owner_of(core, s), False)
 
     run(PLAN[0])
-    split = tiles - tiles // 3
 
     def tick(s):
         for e in range(4):
@@ -532,53 +524,46 @@
             for at, items in PLAN[1].items():
                 if at % 4 == e and at // 4 + 1 <= steps + 1:
                     pl.when(s == at // 4 + 1)(functools.partial(run, items))
-            use(e // 2, s - 1, *((0, split), (split, tiles))[e % 2])
+            if e % 2 == 0:
+                use(e // 2, s - 1)
 
     loop(1, steps + 2, tick)
     for at, items in PLAN[1].items():
         if at // 4 + 1 > steps + 1:
             run(items)
-
-    def sent_so_far():
-        for e in range(2):
-            handover(0, e).wait_send()
-
-        def drain(s):
-            _, used = comes(c, s)
-            for e in range(4):
-                pl.when(goes(s))(lambda e=e: hop(s, e).wait_send())
-                pl.when(used)(lambda e=e: handover(s, e).wait_send())
-
-        loop(1, steps + 1, drain)
-        others(0, n_ep, lambda i: dispatch_copy(i).wait_send())
-        for _, sent in xs + hs:
-            sent()
 
     maps = acc[0:vd, :] / acc[vd : vd + 1, :]
     mixed = maps[:, 0:ta] - scale_ref[0] * maps[:, ta : 2 * ta]
     mean_sq = jnp.mean(mixed * mixed, axis=0, keepdims=True)
     head = (mixed * lax.rsqrt(mean_sq + EPS)).T * hgain_ref[...] * HEAD_FACTOR
     hobuf[:, pl.ds(pl.multiple_of(tp * vd, 128), vd)] = head.astype(BF16)
-    o_stage(0)
-
-    sent_so_far()
-    for i in (1, 30, 2, 31, 32, 33, 5):
-        o_stage(i)
+
+    for what, p, i in PLAN[2]:
+        o_stage(i) if what == "o" else run([(what, p, i)])
     w_copies[3].wait()
     with jax.named_scope("outproj"):
         mixer_ref[...] = dot(hobuf[...], wout[...]).astype(BF16)
 
-    def other_experts(f):
-        loop(1, n_ep, lambda i: f(lax.rem(ep + i, n_ep)))
-
     with jax.named_scope("ret_wait"):
-        other_experts(lambda peer: returned(peer).wait_recv())
+        wait_for(rbuf.at[all_but_one], a2a_recv.at[passes])
     back = rbuf[...]
     weight = [column(rw_ref[i : i + 1, :])[:, 0:1] for i in range(2)]
     mix_ref[...] = (dot(picks[0], back) * weight[0] + dot(picks[1], back) * weight[1]).astype(BF16)
 
-    others(0, n_ep, lambda i: return_copy(i).wait_send())
-    o_sent()
+    with jax.named_scope("drain"):
+        wait_for(chunks(2), pass_send.at[0])
+
+        def drain(s):
+            _, used = comes(c, s)
+            pl.when(goes(s))(lambda: wait_for(chunks(4), ring_send.at[s]))
+            pl.when(used)(lambda: wait_for(chunks(4), pass_send.at[s]))
+
+        loop(1, steps + 1, drain)
+        for i in range(2):
+            wait_for(disp.at[all_but_one], a2a_send.at[i])
+        for _, sent in xs + hs:
+            sent()
+        o_sent()
 
 
 def per_device(nz, ny, nx, *args):
@@ -626,14 +611,14 @@
             pltpu.VMEM(down.shape, BF16),
             pltpu.VMEM(wout.shape, BF16),
             dma((4,)),
+            dma((steps + 1,)),
             dma((steps + 1, 4)),
-            dma((steps + 1, 4)),
-            dma((steps + 1, 4)),
-            dma((steps + 1, 4)),
-            dma((2, n_ep)),
-            dma((2, n_ep)),
-            dma((5, 2, 20)),
-            dma((5, 2, 20)),
+            dma((steps + 1,)),
+            dma((steps + 1,)),
+            dma((2,)),
+            dma((3,)),
+            dma((5,)),
+            dma((5, 7)),
         ],
         compiler_params=pltpu.CompilerParams(
             collective_id=0, has_side_effects=True, vmem_limit_bytes=60 * 1024 * 1024

time: 104 us -> 90.3 us (0.87)
  the two profiles are of different devices: /device:TPU:480 before, /device:TPU:32 now
where the time goes in v3:
time: 90.3 us; the launch traced here: 90.1 us
  Pallas kernels  86.6 us (96%)
  local copies, waits for them, and re-layouts  2.28 us (3%)
  between operations  1.3 us (1%)
    pallas_call x1, Pallas kernels, per_device(): pl.pallas_call(functools.partial(kernel, nz, ny, nx, cap), out_shape=(jax...  86.6 us
    unnamed x4, local copies, waits for them, and re-layouts  2.28 us

profile of v3, /device:TPU:32, one launch (start us, length us, event | category | flops | bytes accessed | tf_op | source)
XLA Modules:
  0.0 90.1 jit_solution(4345571672379523810)
XLA Ops:
  1.3 86.6 %layer.1 = (bf16[384,256]{1,0:T(8,128)(2,1)}, bf16[128,256]{1,0:T(8,128)(2,1)}) custom-call(bf16[384,128]{1,0:T(8,128)(2,1)} %q_ref.1, bf16[384,128]{1,0:T(8,128)(2,1)} %k_ref.1, bf16[384,128]{1,0:T(8,128)(2,1)} %v_ref.1, f32[1]{0:T(128)S(6)} %copy.17.scale_ref, f32[1,128]{1,0:T(1,128)} %bitcast.13, bf16[2048,256]{1,0:T(8,128)(2,1)} %wout_hbm.1, ...), custom_call_target="tpu_custom_call" | custom-call | tf_op jit(solution)/shard_map/layer/pallas_call | solution.py:584
  87.9 0.0 copy-start
  87.9 1.6 %copy.18 = bf16[384,256]{1,0:T(8,128)(2,1)} copy(bf16[384,256]{1,0:T(8,128)(2,1)} %get-tuple-element.4) | data formatting | bytes 393216
  89.5 0.0 copy-done
  89.5 0.6 copy.19
Async XLA Ops:
  87.9 1.7 %copy-start = (bf16[128,256]{1,0:T(8,128)(2,1)S(1)}, bf16[128,256]{1,0:T(8,128)(2,1)}, u32[]{:S(2)}) copy-start(bf16[128,256]{1,0:T(8,128)(2,1)} %get-tuple-element.5) | copy-start | bytes 196612

commit v4 on v3

--- a/solution.py
+++ b/solution.py
@@ -31,17 +31,18 @@
         19: [("h", 0, 1)],
         20: [("h", 0, 11), ("h", 0, 10), ("h", 0, 12)],
         21: [("x", 1, 5)],
-        22: [("h", 0, 2)],
+        22: [("h", 0, 2), ("e", 0, 0)],
         23: [("h", 0, 30)],
-        24: [("h", 0, 31), ("h", 0, 32)],
-        25: [("h", 0, 33)],
+        24: [("h", 0, 31), ("h", 0, 32), ("e", 0, 10)],
+        25: [("h", 0, 33), ("e", 0, 1)],
         26: [("h", 1, 1), ("h", 1, 12), ("h", 1, 10), ("h", 1, 11)],
-        28: [("h", 0, 5)],
-        29: [("h", 1, 2)],
-        30: [("h", 1, 30), ("h", 1, 31)],
-        31: [("h", 1, 32), ("h", 1, 33)],
+        27: [("e", 0, 12)],
+        28: [("h", 0, 5), ("e", 0, 11)],
+        29: [("h", 1, 2), ("e", 0, 2)],
+        30: [("h", 1, 30), ("h", 1, 31), ("e", 0, 30)],
+        31: [("h", 1, 32), ("h", 1, 33), ("e", 0, 32), ("e", 0, 31)],
     },
-    [("o", 0, 0), ("o", 0, 10), ("h", 1, 5), ("o", 0, 1), ("o", 0, 12), ("o", 0, 11), ("o", 0, 2), ("o", 0, 32), ("o", 0, 30), ("o", 0, 31), ("o", 0, 33), ("o", 0, 5)],
+    [("o", 0, 0), ("o", 0, 10), ("h", 1, 5), ("e", 0, 33), ("e", 0, 5), ("o", 0, 1), ("o", 0, 12), ("o", 0, 11), ("o", 0, 2), ("o", 0, 32), ("o", 0, 30), ("o", 0, 31), ("o", 0, 33), ("o", 0, 5)],
 )
 
 
@@ -263,22 +264,21 @@
     def part(owner, core, e):
         return (k_at, v_at)[e % 2](owner, core if e < 2 else 1 - core)
 
-    last = jnp.where(c == 0, steps, nz - 1 - steps)
-    next_chip = jnp.where(c == 0, lax.rem(z + 1, nz), lax.rem(z - 1 + nz, nz))
+    next_chip = jnp.where(c == 1, lax.rem(z + 1, nz), lax.rem(z - 1 + nz, nz))
 
     def owner_of(core, s):
-        return lax.rem(jnp.where(core == 0, z - s + nz, z + s), nz)
+        return lax.rem(jnp.where(core == 1, z - s + nz, z + s), nz)
 
     def comes(core, s):
         low = nz - 2 - steps
         up, down = z - s >= 0, z + s - nz >= 0
-        brought = jnp.where(core == 0, up & (s <= steps), (owner_of(core, s) <= low) & (s <= low + 1))
-        return brought, brought & ((core == 0) | down)
+        brought = jnp.where(core == 1, up & (s <= steps), (owner_of(core, s) <= low) & (s <= low + 1))
+        return brought, brought & ((core == 1) | down)
 
     def goes(s):
         low = nz - 2 - steps
         return jnp.where(
-            c == 0,
+            c == 1,
             (z + 1 < nz) & (z - (s - 1) >= 0) & (s <= steps),
             (owner_of(c, s - 1) <= low) & (s <= low + 1),
         )
@@ -348,12 +348,13 @@
     with jax.named_scope("gain"):
         w_copies[0].wait()
         w_copies[1].wait()
+        w_copies[2].wait()
         gain = gs[...].T
         for i in range(gs.shape[0]):
             rows = slice(128 * i, 128 * (i + 1))
             wgu[rows, :] = (wgu[rows, :].astype(F32) * gain[:, i : i + 1]).astype(BF16)
 
-    def plane_gather(number, rows, block, span):
+    def plane_gather(number, rows, block, span, direct=False):
         quarter = rows // 2
 
         def half_stages(h):
@@ -369,13 +370,15 @@
 
             def send(name, ds, dp, part):
                 group = {"p": 0, "f": 1, "s": 2, "g": 6}[name[0]] + (int(name[2]) if name[0] == "s" else 0)
-                ts, tp_ = {"r": (0, 1), "l": (0, -1), "u": (1, 0), "d": (-1, 0)}[name[1]]
+                ts, tp_ = {"r": (0, 1), "l": (0, -1), "o": (0, 2), "u": (1, 0), "d": (-1, 0)}[name[1]]
                 ref = block(h, index(s + ds, p + dp), *part)
                 remote(
                     ref, ref, xy_send.at[number], xy_recv.at[number, group], {"tp": index(s + ts, p + tp_)}
                 ).start()
 
             def prime():
+                if direct:
+                    send("fo", 0, 0, whole)
                 send("pr", 0, 0, whole)
                 send("pl", 0, 0, whole)
 
@@ -384,8 +387,9 @@
                 send(f"sd{j}", 0, rel[j], whole)
 
             def across():
-                send("fr", 0, -1, low)
-                send("fl", 0, 1, high)
+                if not direct:
+                    send("fr", 0, -1, low)
+                    send("fl", 0, 1, high)
 
             def forward(j):
                 send("gu", -1, rel[j], low)
@@ -439,8 +443,8 @@
         return hobuf.at[pl.ds(0, 2 * rows_a), pl.ds(0, n // 2 * vd)]
 
     xs = [plane_gather(p, rows_x, functools.partial(x_block, p), x_span) for p in range(passes)]
-    hs = [plane_gather(passes + p, rows_x, functools.partial(h_block, p), h_span) for p in range(passes)]
-    o_stage, o_sent = plane_gather(2 * passes, rows_a, ho_block, ho_span)
+    hs = [plane_gather(passes + p, rows_x, functools.partial(h_block, p), h_span, True) for p in range(passes)]
+    o_stage, o_sent = plane_gather(2 * passes, rows_a, ho_block, ho_span, True)
 
     def add_group(p, h, ds):
         at = slice(p * rows_p + h * rows_x, p * rows_p + (h + 1) * rows_x)
@@ -483,13 +487,22 @@
         hs[p][0](i)
         if i == 5:
             at = slice(p * rows_p, (p + 1) * rows_p)
-            if p == 0:
-                w_copies[2].wait()
             with jax.named_scope("down"):
                 obuf[at, :] = dot(hbuf[at, :], wdown[...]).astype(BF16)
             others(2 * nz // passes * p, 2 * nz // passes * (p + 1), lambda j: return_copy(j).start())
             if p == passes - 1:
                 rbuf[rows_of(ep), :] = obuf[rows_of(self_place), :]
+
+    def heads(i):
+        if i == 0:
+            maps = acc[0:vd, :] / acc[vd : vd + 1, :]
+            mixed = maps[:, 0:ta] - scale_ref[0] * maps[:, ta : 2 * ta]
+            mean_sq = jnp.mean(mixed * mixed, axis=0, keepdims=True)
+            head = (mixed * lax.rsqrt(mean_sq + EPS)).T * hgain_ref[...] * HEAD_FACTOR
+            hobuf[:, pl.ds(pl.multiple_of(tp * vd, 128), vd)] = head.astype(BF16)
+        o_stage(i)
+
+    early = nz // 4
 
     def run(items):
         for what, p, i in items:
@@ -499,6 +512,10 @@
                         for ds in (-1, 1):
                             for h in range(2):
                                 add_group(p, h, ds)
+            elif what == "e":
+                pl.when(z < early)(functools.partial(heads, i))
+            elif what == "o":
+                pl.when(z >= early)(functools.partial(heads, i))
             else:
                 (x_stage if what == "x" else h_stage)(p, i)
 
@@ -531,15 +548,8 @@
     for at, items in PLAN[1].items():
         if at // 4 + 1 > steps + 1:
             run(items)
-
-    maps = acc[0:vd, :] / acc[vd : vd + 1, :]
-    mixed = maps[:, 0:ta] - scale_ref[0] * maps[:, ta : 2 * ta]
-    mean_sq = jnp.mean(mixed * mixed, axis=0, keepdims=True)
-    head = (mixed * lax.rsqrt(mean_sq + EPS)).T * hgain_ref[...] * HEAD_FACTOR
-    hobuf[:, pl.ds(pl.multiple_of(tp * vd, 128), vd)] = head.astype(BF16)
-
-    for what, p, i in PLAN[2]:
-        o_stage(i) if what == "o" else run([(what, p, i)])
+    run(PLAN[2])
+
     w_copies[3].wait()
     with jax.named_scope("outproj"):
         mixer_ref[...] = dot(hobuf[...], wout[...]).astype(BF16)

time: 90.3 us -> 88.5 us (0.980)
  the two profiles are of different devices: /device:TPU:32 before, /device:TPU:1 now
where the time goes in v4:
time: 88.5 us; the launch traced here: 86.9 us
  Pallas kernels  83.3 us (94%)
  local copies, waits for them, and re-layouts  2.28 us (3%)
  between operations  1.3 us (1%)
    pallas_call x1, Pallas kernels, per_device(): pl.pallas_call(functools.partial(kernel, nz, ny, nx, cap), out_shape=(jax...  83.3 us
    unnamed x4, local copies, waits for them, and re-layouts  2.28 us

profile of v4, /device:TPU:1, one launch (start us, length us, event | category | flops | bytes accessed | tf_op | source)
XLA Modules:
  0.0 86.9 jit_solution(7769907697507255264)
XLA Ops:
  1.3 83.3 %layer.1 = (bf16[384,256]{1,0:T(8,128)(2,1)}, bf16[128,256]{1,0:T(8,128)(2,1)}) custom-call(bf16[384,128]{1,0:T(8,128)(2,1)} %q_ref.1, bf16[384,128]{1,0:T(8,128)(2,1)} %k_ref.1, bf16[384,128]{1,0:T(8,128)(2,1)} %v_ref.1, f32[1]{0:T(128)S(6)} %copy.17.scale_ref, f32[1,128]{1,0:T(1,128)} %bitcast.13, bf16[2048,256]{1,0:T(8,128)(2,1)} %wout_hbm.1, ...), custom_call_target="tpu_custom_call" | custom-call | tf_op jit(solution)/shard_map/layer/pallas_call | solution.py:594
  84.6 0.0 copy-start
  84.6 1.6 %copy.18 = bf16[384,256]{1,0:T(8,128)(2,1)} copy(bf16[384,256]{1,0:T(8,128)(2,1)} %get-tuple-element.4) | data formatting | bytes 393216
  86.3 0.0 copy-done
  86.3 0.6 copy.19
Async XLA Ops:
  84.6 1.7 %copy-start = (bf16[128,256]{1,0:T(8,128)(2,1)S(1)}, bf16[128,256]{1,0:T(8,128)(2,1)}, u32[]{:S(2)}) copy-start(bf16[128,256]{1,0:T(8,128)(2,1)} %get-tuple-element.5) | copy-start | bytes 196612

commit v5 on v4

--- a/solution.py
+++ b/solution.py
@@ -31,18 +31,18 @@
         19: [("h", 0, 1)],
         20: [("h", 0, 11), ("h", 0, 10), ("h", 0, 12)],
         21: [("x", 1, 5)],
-        22: [("h", 0, 2), ("e", 0, 0)],
+        22: [("h", 0, 2)],
         23: [("h", 0, 30)],
-        24: [("h", 0, 31), ("h", 0, 32), ("e", 0, 10)],
-        25: [("h", 0, 33), ("e", 0, 1)],
-        26: [("h", 1, 1), ("h", 1, 12), ("h", 1, 10), ("h", 1, 11)],
-        27: [("e", 0, 12)],
-        28: [("h", 0, 5), ("e", 0, 11)],
-        29: [("h", 1, 2), ("e", 0, 2)],
-        30: [("h", 1, 30), ("h", 1, 31), ("e", 0, 30)],
-        31: [("h", 1, 32), ("h", 1, 33), ("e", 0, 32), ("e", 0, 31)],
+        24: [("h", 0, 31), ("h", 0, 32)],
+        25: [("h", 1, 1), ("h", 1, 12), ("h", 1, 11), ("h", 1, 10)],
+        26: [("h", 1, 2), ("h", 0, 33)],
+        27: [("e", 0, 0)],
+        28: [("h", 0, 5), ("h", 1, 30)],
+        29: [("h", 1, 31), ("h", 1, 32), ("e", 0, 10)],
+        30: [("h", 1, 33), ("e", 0, 1), ("e", 0, 12), ("e", 0, 11)],
+        31: [("e", 0, 2), ("e", 0, 30)],
     },
-    [("o", 0, 0), ("o", 0, 10), ("h", 1, 5), ("e", 0, 33), ("e", 0, 5), ("o", 0, 1), ("o", 0, 12), ("o", 0, 11), ("o", 0, 2), ("o", 0, 32), ("o", 0, 30), ("o", 0, 31), ("o", 0, 33), ("o", 0, 5)],
+    [("o", 0, 0), ("o", 0, 10), ("h", 1, 5), ("e", 0, 32), ("e", 0, 31), ("e", 0, 33), ("e", 0, 5), ("o", 0, 1), ("o", 0, 12), ("o", 0, 11), ("o", 0, 2), ("o", 0, 32), ("o", 0, 30), ("o", 0, 31), ("o", 0, 33), ("o", 0, 5)],
 )
 
 

time: 88.5 us -> 87.3 us (0.986); the launches traced: 86.9 us -> 87.1 us
  no operation moved by 1% of the time
where the time goes in v5:
time: 87.3 us; the launch traced here: 87.1 us
  Pallas kernels  83.6 us (96%)
  local copies, waits for them, and re-layouts  2.28 us (3%)
  between operations  1.3 us (1%)
    pallas_call x1, Pallas kernels, per_device(): pl.pallas_call(functools.partial(kernel, nz, ny, nx, cap), out_shape=(jax...  83.6 us
    unnamed x4, local copies, waits for them, and re-layouts  2.28 us

profile of v5, /device:TPU:1, one launch (start us, length us, event | category | flops | bytes accessed | tf_op | source)
XLA Modules:
  0.0 87.1 jit_solution(6514257943894371508)
XLA Ops:
  1.3 83.6 %layer.1 = (bf16[384,256]{1,0:T(8,128)(2,1)}, bf16[128,256]{1,0:T(8,128)(2,1)}) custom-call(bf16[384,128]{1,0:T(8,128)(2,1)} %q_ref.1, bf16[384,128]{1,0:T(8,128)(2,1)} %k_ref.1, bf16[384,128]{1,0:T(8,128)(2,1)} %v_ref.1, f32[1]{0:T(128)S(6)} %copy.17.scale_ref, f32[1,128]{1,0:T(1,128)} %bitcast.13, bf16[2048,256]{1,0:T(8,128)(2,1)} %wout_hbm.1, ...), custom_call_target="tpu_custom_call" | custom-call | tf_op jit(solution)/shard_map/layer/pallas_call | solution.py:594
  84.8 0.0 copy-start
  84.8 1.6 %copy.18 = bf16[384,256]{1,0:T(8,128)(2,1)} copy(bf16[384,256]{1,0:T(8,128)(2,1)} %get-tuple-element.4) | data formatting | bytes 393216
  86.5 0.0 copy-done
  86.5 0.6 copy.19
Async XLA Ops:
  84.8 1.7 %copy-start = (bf16[128,256]{1,0:T(8,128)(2,1)S(1)}, bf16[128,256]{1,0:T(8,128)(2,1)}, u32[]{:S(2)}) copy-start(bf16[128,256]{1,0:T(8,128)(2,1)} %get-tuple-element.5) | copy-start | bytes 196612
